TPU v7x, 256 devices: a whole 4x4x8 slice. The times are simulated.
256 devices in a mesh: sp: 32 (over z, x), tp: 8 (over y, core).
Axes of the slice: x: 4, y: 4, z: 8, core: 2. Of those that a mesh axis runs over, the one named last changes fastest.
Arguments:
- residual_signal: bfloat16 [4096, 2048], P('sp', 'tp'), may hold values from -90 to 90
- lifted_signal: bfloat16 [4096, 1024], P('sp', 'tp'), may hold values from -6 to 6
- discrete_timestep: float32 [64, 4096], P('tp', 'sp'), may hold values from 0.17 to 4.2
- additional_log_fading: float32 [64, 4096], P('tp', 'sp'), may hold values from -2.1 to 0
- paired_fading: float32 [2, 32, 64], replicated, may hold values from 4.8828125e-06 to 0.0625
- unpaired_fading: float32 [2, 32, 32], replicated, may hold values from 4.8828125e-06 to 0.0625
- paired_twist: float32 [2, 32, 64], replicated, may hold values from -3.140625 to 3.140625
- unpaired_twist: float32 [2, 32, 32], replicated, may hold values from -3.140625 to 3.140625
- paired_latent_linears: float32 [2, 2, 2, 32, 64, 16], replicated, may hold values from -1 to 1
- unpaired_latent_linears: float32 [2, 2, 2, 32, 32, 16], replicated, may hold values from -1 to 1
- skip_coefficient: float32 [1024], replicated, may hold values from -4 to 4
- closing_norm_multiplier: float32 [1024], replicated, may hold values from 0.1 to 1.9
- emitted_linear: bfloat16 [1024, 2048], replicated, may hold values from -0.1875 to 0.1875
- leading_norm_multiplier: float32 [2048], replicated, may hold values from 0.1 to 1.9
- raising_linear: bfloat16 [2048, 8192], P('sp', 'tp'), may hold values from -0.125 to 0.125
- lowering_linear: bfloat16 [8192, 2048], P('tp', 'sp'), may hold values from -0.0625 to 0.0625
Outputs:
- layer_out: bfloat16 [4096, 2048], P('sp', 'tp')
All inputs are finite; a program needn't handle non-finite values.
Results may differ from a plain program's by a relative error of at most 0.008.
Values may be sent and summed in bfloat16 or wider, within the bound.
A program may use at most 128 MiB of HBM per device.

v0:
```python
import jax
import jax.numpy as jnp
from jax import lax
from jax.sharding import Mesh
from jax.sharding import PartitionSpec as P

D = 2048
CHAN = 16
NORM_W = 128
SP = ("sp_0", "sp_1")


EPSILON = 1e-06


def gather_turned(arrays, axis, dims):
    turned = [jnp.moveaxis(a, dim, 0) for a, dim in zip(arrays, dims)]
    both = jnp.concatenate([t.reshape(len(t), -1) for t in turned], axis=1)
    out, at, outs = (lax.all_gather(both, axis, axis=0, tiled=True), 0, [])
    for t, dim in zip(turned, dims):
        piece = out[:, at : at + t[0].size].reshape(-1, *t.shape[1:])
        outs.append(jnp.moveaxis(piece, 0, dim))
        at += t[0].size
    return tuple(outs)


def neutral_like(array, identity):
    return jax.tree.map(
        lambda part, zero: jnp.zeros_like(part) + jnp.asarray(zero, part.dtype), array, identity
    )


def gathered_once(array, axis):
    leaves = jax.tree.leaves(array)
    order = sorted(range(len(leaves)), key=lambda k: -leaves[k].size)
    width = (1, *leaves[order[0]].shape)[-1]
    lines = [
        jnp.pad(leaves[k].reshape(-1), (0, -leaves[k].size % width)).reshape(-1, width)
        for k in order
    ]
    both, at, found = (lax.all_gather(jnp.concatenate(lines), axis), 0, {})
    for k, line in zip(order, lines):
        piece = both[:, at : at + len(line)].reshape(len(both), -1)
        found[k] = piece[:, : leaves[k].size].reshape(-1, *leaves[k].shape)
        at += len(line)
    numbers = iter(range(len(leaves)))
    return jax.tree.map(lambda _: found[next(numbers)], array)


def carried_in(array, axes, combine, identity):
    before = start = neutral_like(array, identity)
    total = array
    for axis in reversed(axes):
        size, index = (lax.axis_size(axis), lax.axis_index(axis))
        pieces = gathered_once(total, axis)
        inside, total = (start, start)
        for k in range(size):
            passed = k < index
            total = combine(total, jax.tree.map(lambda part: part[k], pieces))
            inside = jax.tree.map(lambda new, old: jnp.where(passed, new, old), total, inside)
        before = combine(inside, before)
    return before


def sent_to_all(array, axis):
    copies = jnp.broadcast_to(array, (lax.axis_size(axis), *array.shape))
    return lax.all_to_all(copies, axis, split_axis=0, concat_axis=0, tiled=True)


def gathered_once_2(array, axis):
    leaves = jax.tree.leaves(array)
    order = sorted(range(len(leaves)), key=lambda k: -leaves[k].size)
    width = (1, *leaves[order[0]].shape)[-1]
    lines = [
        jnp.pad(leaves[k].reshape(-1), (0, -leaves[k].size % width)).reshape(-1, width)
        for k in order
    ]
    both, at, found = (sent_to_all(jnp.concatenate(lines), axis), 0, {})
    for k, line in zip(order, lines):
        piece = both[:, at : at + len(line)].reshape(len(both), -1)
        found[k] = piece[:, : leaves[k].size].reshape(-1, *leaves[k].shape)
        at += len(line)
    numbers = iter(range(len(leaves)))
    return jax.tree.map(lambda _: found[next(numbers)], array)


def combined_pairwise(pieces, combine):
    while len(jax.tree.leaves(pieces)[0]) > 1:
        pieces = jax.vmap(combine)(
            *(jax.tree.map(lambda part: part[side::2], pieces) for side in (0, 1))
        )
    return jax.tree.map(lambda part: part[0], pieces)


def prefix(array, axis, combine, identity):
    size, index = (lax.axis_size(axis), lax.axis_index(axis))
    passed = jnp.arange(size) > index

    def kept(part, zero, own):
        part = jnp.where(
            passed.reshape(-1, *(1 for _ in own.shape)), part, jnp.asarray(zero, own.dtype)
        )
        return part[::-1]

    pieces = gathered_once_2(array, axis)
    return combined_pairwise(jax.tree.map(kept, pieces, identity, array), combine)


def of_everyone(array, axis):
    return sent_to_all(array, axis).sum(axis=0)


def joined_along(blocks, dim):
    blocks = jnp.moveaxis(blocks, 0, dim)
    shape = blocks.shape
    return blocks.reshape(*shape[:dim], shape[dim] * shape[dim + 1], *shape[dim + 2 :])


def gather_directly(array, axis, dim):
    return joined_along(sent_to_all(array, axis), dim)


def in_blocks(array, dim, size):
    shape = array.shape
    blocks = array.reshape(*shape[:dim], size, shape[dim] // size, *shape[dim + 1 :])
    return jnp.moveaxis(blocks, dim, 0)


def sent_and_summed(array, axis, dim):
    blocks = in_blocks(array, dim, lax.axis_size(axis))
    arrived = lax.all_to_all(blocks, axis, split_axis=0, concat_axis=0, tiled=True)
    return arrived.astype(jnp.float32).sum(axis=0)


def combine_maps(early, later):
    first_re, first_im, base_re, base_im = early
    next_re, next_im, add_re, add_im = later
    return (
        next_re * first_re - next_im * first_im,
        next_re * first_im + next_im * first_re,
        next_re * base_re - next_im * base_im + add_re,
        next_re * base_im + next_im * base_re + add_im,
    )


def one_kind_map(weights, reading):
    groups, states, channels = weights.shape
    diagonal_ones = jnp.eye(groups, dtype=jnp.float32)
    if reading:
        return jnp.einsum("gh,gpj->gphj", diagonal_ones, weights).reshape(
            groups * states, groups * channels
        )
    return jnp.einsum("gh,gpj->gjhp", diagonal_ones, weights).reshape(
        groups * channels, groups * states
    )


def block_map(long_weights, short_weights, reading):
    long_part = one_kind_map(long_weights, reading)
    short_part = one_kind_map(short_weights, reading)
    upper = jnp.concatenate(
        [long_part, jnp.zeros((long_part.shape[0], short_part.shape[1]), jnp.float32)], axis=1
    )
    lower = jnp.concatenate(
        [jnp.zeros((short_part.shape[0], long_part.shape[1]), jnp.float32), short_part], axis=1
    )
    return jnp.concatenate([upper, lower], axis=0)


def on_device(
    residual_signal,
    lifted_signal,
    discrete_timestep,
    additional_log_fading,
    paired_fading,
    unpaired_fading,
    paired_twist,
    unpaired_twist,
    paired_latent_linears,
    unpaired_latent_linears,
    skip_coefficient,
    closing_norm_multiplier,
    emitted_linear,
    leading_norm_multiplier,
    raising_linear,
    lowering_linear,
):
    up_whole, down_whole = gather_turned((raising_linear, lowering_linear), SP, (0, 1))
    rank = lax.axis_index("tp")
    batch_number = residual_signal.shape[0]
    local_groups = discrete_timestep.shape[0]
    midpoint_extent = local_groups // 2
    width = lifted_signal.shape[1]
    long_states = paired_fading.shape[2]
    short_states = unpaired_fading.shape[2]

    def owned(array, axis, count):
        return lax.dynamic_slice_in_dim(array, rank * count, count, axis)

    grouped = lifted_signal.astype(jnp.float32).reshape(batch_number, midpoint_extent, 2, CHAN)
    flat_inputs = jnp.concatenate(
        [grouped[:, :, 0].reshape(batch_number, -1), grouped[:, :, 1].reshape(batch_number, -1)],
        axis=1,
    )
    pace = discrete_timestep.T.reshape(batch_number, midpoint_extent, 2)
    surge_entries = additional_log_fading.T.reshape(batch_number, midpoint_extent, 2)

    def spread_out(values):
        long_part = jnp.broadcast_to(
            values[:, :, 0][:, :, None], (batch_number, midpoint_extent, long_states)
        )
        short_part = jnp.broadcast_to(
            values[:, :, 1][:, :, None], (batch_number, midpoint_extent, short_states)
        )
        return jnp.concatenate(
            [long_part.reshape(batch_number, -1), short_part.reshape(batch_number, -1)], axis=1
        )

    pace_flat = spread_out(pace)
    surge_flat = spread_out(surge_entries)
    long_linears = owned(paired_latent_linears, 3, midpoint_extent)
    short_linears = owned(unpaired_latent_linears, 3, midpoint_extent)

    def flat_rates(direction, long_array, short_array):
        return jnp.concatenate(
            [
                owned(long_array, 1, midpoint_extent)[direction].reshape(-1),
                owned(short_array, 1, midpoint_extent)[direction].reshape(-1),
            ]
        )

    def scanned(direction, backward):
        decay_rate = flat_rates(direction, paired_fading, unpaired_fading)[None]
        turn_rate = flat_rates(direction, paired_twist, unpaired_twist)[None]
        magnitude = jnp.exp(-decay_rate * pace_flat + surge_flat)
        angle = turn_rate * pace_flat
        weight_in = jnp.sqrt(-jnp.expm1(-2.0 * decay_rate * pace_flat))
        drive_re = (
            jnp.dot(
                flat_inputs,
                block_map(long_linears[direction, 0, 0], short_linears[direction, 0, 0], False),
                precision=lax.Precision.HIGHEST,
            )
            * weight_in
        )
        drive_im = (
            jnp.dot(
                flat_inputs,
                block_map(long_linears[direction, 0, 1], short_linears[direction, 0, 1], False),
                precision=lax.Precision.HIGHEST,
            )
            * weight_in
        )
        maps = (magnitude * jnp.cos(angle), magnitude * jnp.sin(angle), drive_re, drive_im)
        return lax.associative_scan(combine_maps, maps, reverse=backward, axis=0)

    def settle(maps, arriving, direction):
        prefix_re, prefix_im, state_re, state_im = maps
        carry_re, carry_im = arriving
        state_re = state_re + prefix_re * carry_re[None] - prefix_im * carry_im[None]
        state_im = state_im + prefix_re * carry_im[None] + prefix_im * carry_re[None]
        read_re = block_map(long_linears[direction, 1, 0], short_linears[direction, 1, 0], True)
        read_im = block_map(long_linears[direction, 1, 1], short_linears[direction, 1, 1], True)
        return jnp.dot(state_re, read_re, precision=lax.Precision.HIGHEST) - jnp.dot(
            state_im, read_im, precision=lax.Precision.HIGHEST
        )

    state_count = pace_flat.shape[1]
    blank = jnp.zeros((state_count,), jnp.float32)
    identity = (jnp.ones((state_count,), jnp.float32), blank, blank, blank)
    forward_maps = scanned(0, False)
    forward_ends = tuple((member[-1] for member in forward_maps))
    from_before = carried_in(forward_ends, SP, combine_maps, identity)
    backward_maps = scanned(1, True)
    backward_ends = tuple((member[0] for member in backward_maps))
    from_after = prefix(backward_ends, SP, combine_maps, identity)
    kind_major = settle(forward_maps, from_before[2:4], 0) + settle(
        backward_maps, from_after[2:4], 1
    )
    ssm_out = (
        kind_major.reshape(batch_number, 2, midpoint_extent, CHAN)
        .transpose(0, 2, 1, 3)
        .reshape(batch_number, width)
    )
    activated = jax.nn.gelu(
        ssm_out + owned(skip_coefficient, 0, width)[None] * grouped.reshape(batch_number, width)
    )
    heads = activated.reshape(batch_number, width // NORM_W, NORM_W)
    heads = heads * lax.rsqrt(jnp.mean(heads * heads, axis=2, keepdims=True) + EPSILON)
    combined_result = (
        heads.reshape(batch_number, width) * owned(closing_norm_multiplier, 0, width)[None]
    ).astype(jnp.bfloat16)
    position_rows = lax.all_to_all(combined_result, "tp", split_axis=0, concat_axis=1, tiled=True)
    projected = jnp.dot(position_rows, emitted_linear, preferred_element_type=jnp.float32)
    blended_result = lax.all_to_all(
        projected.astype(jnp.bfloat16), "tp", split_axis=1, concat_axis=0, tiled=True
    ).astype(projected.dtype)
    hidden_activity = residual_signal.shape[1]
    inner_activity = residual_signal.astype(jnp.float32) + blended_result
    squares = of_everyone(jnp.sum(inner_activity * inner_activity, axis=1), "tp")
    scale = lax.rsqrt(squares / D + EPSILON)
    normed = (
        inner_activity * scale[:, None] * owned(leading_norm_multiplier, 0, hidden_activity)[None]
    ).astype(jnp.bfloat16)
    whole_rows = gather_directly(normed, "tp", 1)
    upward = jnp.dot(whole_rows, up_whole, preferred_element_type=jnp.float32)
    hidden = jnp.square(jax.nn.relu(upward)).astype(jnp.bfloat16)
    partial_value = jnp.dot(hidden, down_whole, preferred_element_type=jnp.float32)
    feed = sent_and_summed(partial_value.astype(jnp.bfloat16), "tp", 1)
    return (inner_activity + feed).astype(jnp.bfloat16)


def solution(mesh):
    split = Mesh(mesh.devices.reshape(8, 4, mesh.shape["tp"]), ("sp_0", "sp_1", "tp"))
    return jax.shard_map(
        on_device,
        mesh=split,
        in_specs=(
            P(SP, "tp"),
            P(SP, "tp"),
            P("tp", SP),
            P("tp", SP),
            P(),
            P(),
            P(),
            P(),
            P(),
            P(),
            P(),
            P(),
            P(),
            P(),
            P(SP, "tp"),
            P("tp", SP),
        ),
        out_specs=P(SP, "tp"),
        check_vma=False,
    )
```

profile of v0, /device:TPU:1, one launch (start us, length us, event | category | flops | bytes accessed | tf_op | source)
XLA Modules:
  0.0 203.1 jit_solution(7310066196905179590)
XLA Ops:
  6.5 0.9 dynamic-slice_bitcast_fusion.1
  7.7 1.0 multiply_bitcast_fusion.1
  8.9 0.9 dynamic-slice_bitcast_fusion
  10.0 1.0 multiply_bitcast_fusion
  11.2 0.8 constant_dynamic-slice_fusion.5
  12.0 0.7 constant_dynamic-slice_fusion.4
  15.1 0.7 cosine_multiply_fusion
  21.4 0.7 broadcast_in_dim.99
  22.1 12.0 %all-to-all-start = ((f32[32,4,384]{2,1,0:T(4,128)}), f32[32,4,384]{2,1,0:T(4,128)}, u32[]{:S(2)}, u32[]{:S(2)}) async-start(f32[32,4,384]{2,1,0:T(4,128)} %broadcast_in_dim.99), calls=%async_computation | async-start | bytes 393216 | tf_op jit(solution)/shard_map/all_to_all | solution.py:67
  34.3 0.8 pad_maximum_fusion
  37.3 0.7 cosine_multiply_fusion.1
  38.1 0.7 slice.1390
  38.8 0.7 slice.1384
  39.4 0.7 slice.1391
  40.1 1.0 multiply_subtract_fusion.3
  41.3 0.6 slice.1397
  41.9 0.6 slice.1406
  42.5 0.8 add_add_fusion.7
  44.0 0.6 slice.1434
  47.6 0.6 slice.1437
  54.2 1.3 slice.1457
  55.5 1.3 slice.1461
  56.8 1.2 slice.1807
  58.1 1.3 slice.1784
  62.2 0.6 slice.1473
  63.9 0.6 slice.1479
  65.7 0.7 slice.1481
  66.4 0.7 slice.1512
  67.0 0.7 add_add_fusion.25
  67.9 0.7 multiply_add_fusion.32
  68.6 1.4 slice_add_fusion.64
  70.2 0.7 multiply_add_fusion.21
  70.9 0.6 pad_maximum_fusion.43
  71.6 0.6 pad_maximum_fusion.42
  72.2 0.7 multiply_add_fusion.16
  73.0 0.7 pad_maximum_fusion.35
  73.7 0.7 pad_maximum_fusion.34
  74.8 0.7 pad_maximum_fusion.14
  76.7 0.6 add_add_fusion.6
  77.4 0.6 pad_maximum_fusion.12
  78.1 0.8 pad_maximum_fusion.13
  79.0 1.6 add_add_fusion.2
  80.7 0.9 pad_maximum_fusion.6
  81.7 1.0 reshape.1448
  82.7 1.0 reshape.1449
  83.8 9.7 %all-gather.2 = f32[4,4,384]{2,1,0:T(4,128)S(1)} all-gather(f32[1,4,384]{2,1,0:T(4,128)S(1)} %maximum_bitcast_fusion), channel_id=2, replica_groups=mesh['sp_0'=8,'sp_1'=4,'tp'=8] {'sp_1'}, dimensions={0}, use_global_device_ids=true | all-gather | bytes 30720 | tf_op jit(solution)/shard_map/all_gather | solution.py:41
  93.6 22.0 %all-gather.3 = f32[8,4,384]{2,1,0:T(4,128)S(1)} all-gather(f32[1,4,384]{2,1,0:T(4,128)S(1)} %maximum_bitcast_fusion.1), channel_id=3, replica_groups=mesh['sp_0'=8,'sp_1'=4,'tp'=8] {'sp_0'}, dimensions={0}, use_global_device_ids=true | all-gather | bytes 55296 | tf_op jit(solution)/shard_map/all_gather | solution.py:41
  116.0 1.1 fusion.36
  117.7 1.0 reshape.1460
  118.8 1.0 reshape.1450
  120.2 0.8 dynamic_slice.37
  121.0 0.8 dynamic_slice.38
  121.8 1.3 convolution_subtract_fusion.1
  123.1 1.6 fusion.156
  127.4 16.9 %all_to_all.50 = bf16[8,16,128]{2,1,0:T(8,128)(2,1)S(1)} all-to-all(bf16[8,16,128]{2,1,0:T(8,128)(2,1)S(1)} %multiply_convert_fusion.1), channel_id=1, replica_groups=mesh['sp_0'=8,'sp_1'=4,'tp'=8] {'tp'}, dimensions={0} | all-to-all | bytes 65536 | tf_op jit(solution)/shard_map/all_to_all | solution.py:293
  144.4 2.8 %convolution_convert_fusion = bf16[16,2048]{1,0:T(8,128)(2,1)S(1)} fusion(bf16[1024,2048]{1,0:T(8,128)(2,1)} %param.28, bf16[8,16,128]{2,1,0:T(8,128)(2,1)S(1)} %all_to_all.50), kind=kOutput, calls=%fused_computation.5 | convolution fusion | flops 67141632 | bytes 4292608 | tf_op jit(solution)/shard_map/dot_general | solution.py:294
  147.2 8.0 %all_to_all.51 = bf16[16,8,256]{2,0,1:T(8,128)(2,1)S(1)} all-to-all(bf16[16,8,256]{2,0,1:T(8,128)(2,1)S(1)} %bitcast.357), channel_id=1, replica_groups=mesh['sp_0'=8,'sp_1'=4,'tp'=8] {'tp'}, dimensions={1} | all-to-all | bytes 131072 | tf_op jit(solution)/shard_map/all_to_all | solution.py:295
  155.9 4.0 %all-to-all-start.3 = ((f32[8,1,128]{2,1,0:T(1,128)}), f32[8,1,128]{2,1,0:T(1,128)S(1)}, u32[]{:S(2)}, u32[]{:S(2)}) async-start(f32[8,1,128]{2,1,0:T(1,128)} %broadcast_in_dim.102), calls=%async_computation.3 | async-start | bytes 8192 | tf_op jit(solution)/shard_map/all_to_all | solution.py:67
  159.9 0.8 dynamic_slice.39
  160.6 3.8 %all-to-all-done.3 = f32[8,1,128]{2,1,0:T(1,128)S(1)} async-done(((f32[8,1,128]{2,1,0:T(1,128)}), f32[8,1,128]{2,1,0:T(1,128)S(1)}, u32[]{:S(2)}, u32[]{:S(2)}) %all-to-all-start.3) | async-done | bytes 4128 | tf_op jit(solution)/shard_map/all_to_all | solution.py:67
  164.7 12.4 %all_to_all.52 = bf16[8,128,256]{1,2,0:T(8,128)(2,1)S(1)} all-to-all(bf16[8,128,256]{1,2,0:T(8,128)(2,1)S(1)} %broadcast_in_dim.103), channel_id=1, replica_groups=mesh['sp_0'=8,'sp_1'=4,'tp'=8] {'tp'}, dimensions={0} | all-to-all | bytes 1048576 | tf_op jit(solution)/shard_map/all_to_all | solution.py:67
  177.2 5.6 %fusion.4 = bf16[128,2048]{1,0:T(8,128)(2,1)S(1)} fusion(bf16[2048,2048]{1,0:T(8,128)(2,1)} %all-gather.6.cloned.1.call-done, bf16[128,2048]{0,1:T(8,128)(2,1)S(1)} %bitcast.348), kind=kOutput, calls=%fused_computation.4 | convolution fusion | flops 1074397184 | bytes 9437184 | tf_op jit(solution)/shard_map/dot_general | solution.py:308
  182.8 12.8 %all_to_all.53 = bf16[8,128,256]{2,1,0:T(8,128)(2,1)S(1)} all-to-all(bf16[8,128,256]{2,1,0:T(8,128)(2,1)S(1)} %bitcast.346), channel_id=1, replica_groups=mesh['sp_0'=8,'sp_1'=4,'tp'=8] {'tp'}, dimensions={0} | all-to-all | bytes 1048576 | tf_op jit(solution)/shard_map/all_to_all | solution.py:131
  195.6 0.7 add_convert_fusion
  (655 shorter events, 30.8 us)
Async XLA Ops:
  6.5 6.4 %copy-start.43 = (f32[8,128]{1,0:T(8,128)S(1)}, f32[8,128]{1,0:T(8,128)}, u32[]{:S(2)}) copy-start(f32[8,128]{1,0:T(8,128)} %param.18) | copy-start | bytes 12292
  6.5 6.6 %copy-start.21 = (bf16[128,128]{1,0:T(8,128)(2,1)S(1)}, bf16[128,128]{1,0:T(8,128)(2,1)}, u32[]{:S(2)}) copy-start(bf16[128,128]{1,0:T(8,128)(2,1)} %param.17) | copy-start | bytes 98308
  7.6 7.2 %copy-start.44 = (f32[8,128]{1,0:T(8,128)S(1)}, f32[8,128]{1,0:T(8,128)}, u32[]{:S(2)}) copy-start(f32[8,128]{1,0:T(8,128)} %param.19) | copy-start | bytes 12292
  20.0 14.2 %copy-start.6 = (bf16[1024,64]{0,1:T(8,128)(2,1)S(1)}, bf16[1024,64]{0,1:T(8,128)(2,1)}, u32[]{:S(2)}) copy-start(bf16[1024,64]{0,1:T(8,128)(2,1)} %param.31) | copy-start | bytes 393220
  20.0 14.2 %copy-start.7 = (bf16[64,1024]{1,0:T(8,128)(2,1)S(1)}, bf16[64,1024]{1,0:T(8,128)(2,1)}, u32[]{:S(2)}) copy-start(bf16[64,1024]{1,0:T(8,128)(2,1)} %param.30) | copy-start | bytes 393220
  22.1 101.0 %all-to-all-start = ((f32[32,4,384]{2,1,0:T(4,128)}), f32[32,4,384]{2,1,0:T(4,128)}, u32[]{:S(2)}, u32[]{:S(2)}) async-start(f32[32,4,384]{2,1,0:T(4,128)} %broadcast_in_dim.99), calls=%async_computation | async-start | bytes 393216 | tf_op jit(solution)/shard_map/all_to_all | solution.py:67
  34.0 143.1 %all-gather.6.cloned.1.call-start = ((), (), s32[]{:S(2)}) async-start(), calls=%async_computation.6 | async-start | bytes 8650752 | tf_op jit(solution)/shard_map/all_gather | solution.py:19
  36.1 30.9 %copy-start.3 = (f32[128,384]{1,0:T(8,128)}, f32[128,384]{1,0:T(8,128)S(1)}, u32[]{:S(2)}) copy-start(f32[128,384]{1,0:T(8,128)S(1)} %convolution_multiply_fusion.3) | copy-start | bytes 589828
  37.0 37.4 %copy-start.4 = (f32[128,384]{1,0:T(8,128)}, f32[128,384]{1,0:T(8,128)S(1)}, u32[]{:S(2)}) copy-start(f32[128,384]{1,0:T(8,128)S(1)} %convolution_multiply_fusion.2) | copy-start | bytes 589828
  43.7 9.8 %copy-start.12 = (f32[8,384]{1,0:T(8,128)}, f32[8,384]{1,0:T(8,128)S(1)}, u32[]{:S(2)}) copy-start(f32[8,384]{1,0:T(8,128)S(1)} %get-tuple-element.168) | copy-start | bytes 36868
  43.7 9.8 %copy-start.13 = (f32[8,384]{1,0:T(8,128)}, f32[8,384]{1,0:T(8,128)S(1)}, u32[]{:S(2)}) copy-start(f32[8,384]{1,0:T(8,128)S(1)} %get-tuple-element.167) | copy-start | bytes 36868
  43.9 8.9 %copy-start.17 = (f32[4,384]{1,0:T(4,128)}, f32[4,384]{1,0:T(4,128)S(1)}, u32[]{:S(2)}) copy-start(f32[4,384]{1,0:T(4,128)S(1)} %get-tuple-element.208) | copy-start | bytes 18436
  43.9 9.6 %copy-start.18 = (f32[4,384]{1,0:T(4,128)}, f32[4,384]{1,0:T(4,128)S(1)}, u32[]{:S(2)}) copy-start(f32[4,384]{1,0:T(4,128)S(1)} %get-tuple-element.209) | copy-start | bytes 18436
  43.9 9.6 %copy-start.19 = (f32[4,384]{1,0:T(4,128)}, f32[4,384]{1,0:T(4,128)S(1)}, u32[]{:S(2)}) copy-start(f32[4,384]{1,0:T(4,128)S(1)} %get-tuple-element.240) | copy-start | bytes 18436
  43.9 9.6 %copy-start.20 = (f32[4,384]{1,0:T(4,128)}, f32[4,384]{1,0:T(4,128)S(1)}, u32[]{:S(2)}) copy-start(f32[4,384]{1,0:T(4,128)S(1)} %get-tuple-element.241) | copy-start | bytes 18436
  54.2 21.5 %copy-start.32 = (f32[1,384]{1,0:T(1,128)S(1)}, f32[1,384]{1,0:T(1,128)}, u32[]{:S(2)}) copy-start(f32[1,384]{1,0:T(1,128)} %slice.1825) | copy-start | bytes 4612
  67.0 9.7 %copy-start.5 = (f32[31,384]{1,0:T(8,128)S(1)}, f32[31,384]{1,0:T(8,128)}, u32[]{:S(2)}) copy-start(f32[31,384]{1,0:T(8,128)} %slice.1479) | copy-start | bytes 142852
  67.8 2.4 %copy-start.30 = (f32[1,384]{1,0:T(1,128)}, f32[1,384]{1,0:T(1,128)S(1)}, u32[]{:S(2)}) copy-start(f32[1,384]{1,0:T(1,128)S(1)} %slice.1787) | copy-start | bytes 4612
  67.8 2.2 %copy-start.24 = (f32[1,384]{1,0:T(1,128)}, f32[1,384]{1,0:T(1,128)S(1)}, u32[]{:S(2)}) copy-start(f32[1,384]{1,0:T(1,128)S(1)} %get-tuple-element.235) | copy-start | bytes 4612
  67.8 2.3 %copy-start.26 = (f32[1,384]{1,0:T(1,128)}, f32[1,384]{1,0:T(1,128)S(1)}, u32[]{:S(2)}) copy-start(f32[1,384]{1,0:T(1,128)S(1)} %get-tuple-element.234) | copy-start | bytes 4612
  67.8 2.3 %copy-start.28 = (f32[1,384]{1,0:T(1,128)}, f32[1,384]{1,0:T(1,128)S(1)}, u32[]{:S(2)}) copy-start(f32[1,384]{1,0:T(1,128)S(1)} %get-tuple-element.262) | copy-start | bytes 4612
  74.4 1.5 copy-start.41
  74.4 1.5 copy-start.42
  74.5 1.5 copy-start.27
  74.5 1.5 copy-start.29
  74.5 1.5 copy-start.39
  74.5 1.5 copy-start.40
  74.5 1.6 copy-start.25
  74.5 1.6 copy-start.31
  74.5 1.6 copy-start.14
  74.5 1.6 copy-start.22
  74.5 1.6 copy-start.23
  74.5 1.7 copy-start.38
  74.6 1.7 copy-start.37
  74.6 1.8 copy-start.8
  74.6 1.8 copy-start.9
  74.6 1.8 copy-start.15
  74.6 1.8 copy-start.16
  74.6 1.8 copy-start.36
  74.6 1.8 copy-start.35
  74.6 1.9 copy-start.10
  74.6 1.9 copy-start.11
  74.6 1.9 copy-start.34
  74.7 2.0 copy-start.33
  75.5 5.1 %slice-start = ((f32[128,384]{1,0:T(8,128)}), f32[1,384]{1,0:T(1,128)S(1)}, s32[]{:S(2)}) async-start(f32[128,384]{1,0:T(8,128)} %copy-done.3), calls=%async_computation.7 | async-start | bytes 3072 | tf_op jit(solution)/shard_map/slice | solution.py:255
  75.6 5.0 %slice-start.1 = ((f32[128,384]{1,0:T(8,128)}), f32[1,384]{1,0:T(1,128)S(1)}, s32[]{:S(2)}) async-start(f32[128,384]{1,0:T(8,128)} %copy-done.4), calls=%async_computation.8 | async-start | bytes 3072 | tf_op jit(solution)/shard_map/slice | solution.py:255
  117.1 1.6 copy-start.1
  117.1 2.9 %copy-start.2 = (f32[4,64,4,16]{1,0,3,2:T(4,128)S(1)}, f32[4,64,4,16]{1,0,3,2:T(4,128)}, u32[]{:S(2)}) copy-start(f32[4,64,4,16]{1,0,3,2:T(4,128)} %get-tuple-element.264) | copy-start | bytes 196612
  124.8 30.3 %copy-start = (bf16[128,256]{1,0:T(8,128)(2,1)S(1)}, bf16[128,256]{1,0:T(8,128)(2,1)}, u32[]{:S(2)}) copy-start(bf16[128,256]{1,0:T(8,128)(2,1)} %param.16) | copy-start | bytes 196612
  155.9 8.5 %all-to-all-start.3 = ((f32[8,1,128]{2,1,0:T(1,128)}), f32[8,1,128]{2,1,0:T(1,128)S(1)}, u32[]{:S(2)}, u32[]{:S(2)}) async-start(f32[8,1,128]{2,1,0:T(1,128)} %broadcast_in_dim.102), calls=%async_computation.3 | async-start | bytes 8192 | tf_op jit(solution)/shard_map/all_to_all | solution.py:67
Sparse Core Ops, SparseCore 0:
  37.4 99.5 all-gather.5
where the time goes:
time: 205 us; the launch traced here: 203 us
  blocking collectives  81.8 us (40%)
  local copies, waits for them, and re-layouts  49.7 us (24%)
  other arithmetic  21.6 us (11%)
  between operations  16.8 us (8%)
  starting transfers between devices  16.2 us (8%)
  matrix products  13.2 us (6%)
  waiting for transfers between devices  3.81 us (2%)
    all_gather x2, blocking collectives, gathered_once(): both, at, found = (lax.all_gather(jnp.concatenate(lines), axis), 0, {})  31.8 us
    slice x196, local copies, waits for them, and re-layouts, scanned(): return lax.associative_scan(combine_maps, maps, reverse=backward, axis=0)  29.8 us
    all_to_all x1, blocking collectives, on_device(): lax.all_to_all(combined_result, 'tp', split_axis=0, concat_axis=1, tiled=...  16.9 us
    all_to_all x2, starting transfers between devices, sent_to_all(): return lax.all_to_all(copies, axis, split_axis=0, concat_axis=0, tiled=True)  16 us
    all_to_all x1, blocking collectives, sent_and_summed(): lax.all_to_all(blocks, axis, split_axis=0, concat_axis=0, tiled=True)  12.8 us
    all_to_all x1, blocking collectives, sent_to_all(): return lax.all_to_all(copies, axis, split_axis=0, concat_axis=0, tiled=True)  12.4 us
    all_to_all x1, blocking collectives, on_device(): lax.all_to_all(projected.astype(jnp.bfloat16), 'tp', split_axis=1, concat...  7.95 us
    concatenate x48, other arithmetic, scanned(): return lax.associative_scan(combine_maps, maps, reverse=backward, axis=0)  6.03 us
  transfers between devices with their start and end apart: 3, of which 1 were waited for; matrix products, arithmetic and copies ran while one was open for 32% of the time, Pallas kernels for 0%

commit v1 on v0

v1 whole, which is shorter than its diff:
```python
import jax
import jax.numpy as jnp
from jax import lax
from jax.experimental import pallas as pl
from jax.experimental.pallas import tpu as pltpu
from jax.sharding import PartitionSpec as P

F32 = jnp.float32
BF16 = jnp.bfloat16
HI = lax.Precision.HIGHEST
MESH = pl.DeviceIdType.MESH
EPSILON = 1e-6

NX, NY, NZ = 4, 4, 8
TOK = 128
CH = 128
ST = 384
LONG = 256
D = 2048
STEPS = 16
CHUNKS = 8


def iota(shape, dim):
    return lax.broadcasted_iota(jnp.int32, shape, dim)


def one_hot(pred):
    return jnp.where(pred, 1.0, 0.0).astype(F32)


def nt(a, b, precision=None):
    return lax.dot_general(
        a, b, (((1,), (1,)), ((), ())), precision=precision, preferred_element_type=F32
    )


def mm(a, b, precision=None):
    return jnp.dot(a, b, precision=precision, preferred_element_type=F32)


def sincos(a):
    k = jnp.floor(a * 0.6366197723675814 + 0.5)
    r = ((a - k * 1.5703125) - k * 4.837512969970703125e-4) - k * 7.549789948768648e-8
    z = r * r
    s = ((-1.9515295891e-4 * z + 8.3321608736e-3) * z - 1.6666654611e-1) * z * r + r
    c = ((2.443315711809948e-5 * z - 1.388731625493765e-3) * z + 4.166664568298827e-2) * z * z
    c = c - 0.5 * z + 1.0
    half = jnp.floor(k * 0.5)
    odd = (k - 2.0 * half) > 0.5
    low = half - 2.0 * jnp.floor(half * 0.5)
    sin_sign = 1.0 - 2.0 * low
    cos_sign = jnp.where(odd, -sin_sign, sin_sign)
    return jnp.where(odd, c, s) * sin_sign, jnp.where(odd, s, c) * cos_sign


def lost(u):
    poly = 1.0 - u * (1.0 / 8)
    for n in (7, 6, 5, 4, 3, 2):
        poly = 1.0 - u * poly * (1.0 / n)
    return jnp.where(u < 0.6, u * poly, 1.0 - jnp.exp(-u))


def kernel(
    residual, lifted, pace, fading, rate_l, rate_s, turn_l, turn_s, proj_l, proj_s,
    skip, closing, emitted, leading, raising, lowering,
    out,
    lifted_v, pace_v, fading_v, rate_lv, rate_sv, turn_lv, turn_sv, proj_lv, proj_sv,
    skip_v, closing_v, emitted_v, leading_v,
    maps_v, pace_s, fading_s, drive_s, prefix_s, state_s, lifted_s,
    ends, cx, cz, row_ends, merged_v, gathered, res_v, mid_v, mid_f, own_mid,
    weights, hidden, partial, arrived,
    load_sem, up_send, up_recv, down_send, down_recv, cx_send, cx_recv, cz_send, cz_recv,
    mg_send, mg_recv, rs_send, rs_recv, res_send, res_recv, ring_send, ring_recv,
    sib_send, sib_recv, mid_send, mid_recv,
):
    sp = lax.axis_index("sp")
    tp = lax.axis_index("tp")
    z, x = sp // NX, sp % NX
    y, c = tp // 2, tp % 2
    sib = y * 2 + (1 - c)
    chip = x * NY + y
    block = x // 2
    inner = x % 2

    def remote(src, dst, send, recv, to):
        return pltpu.make_async_remote_copy(
            src_ref=src, dst_ref=dst, send_sem=send, recv_sem=recv,
            device_id=to, device_id_type=MESH,
        )

    def arrival(ref, sem):
        pltpu.make_async_copy(ref, ref, sem).wait()

    barrier = pltpu.get_barrier_semaphore()
    spot = x * 8 + tp

    @pl.loop(1, 32)
    def _(off):
        to = (spot + off) % 32
        pl.semaphore_signal(barrier, inc=1, device_id=(z * NX + to // 8, to % 8), device_id_type=MESH)

    @pl.loop(1, NZ)
    def _(off):
        pl.semaphore_signal(
            barrier, inc=1, device_id=(((z + off) % NZ) * NX + x, tp), device_id_type=MESH
        )

    loads = [
        (lifted, lifted_v), (pace, pace_v), (fading, fading_v), (rate_l, rate_lv),
        (rate_s, rate_sv), (turn_l, turn_lv), (turn_s, turn_sv),
        (proj_l.at[:, :, :, pl.ds(tp * 4, 4)], proj_lv),
        (proj_s.at[:, :, :, pl.ds(tp * 4, 4)], proj_sv),
        (skip, skip_v), (closing, closing_v), (leading, leading_v), (emitted, emitted_v),
    ]
    copies = [pltpu.make_async_copy(a, b, load_sem.at[n]) for n, (a, b) in enumerate(loads)]
    for copy in copies:
        copy.start()
    for copy in copies[:-1]:
        copy.wait()

    r2, t2 = iota((TOK, TOK), 0), iota((TOK, TOK), 1)
    perm = one_hot(t2 == (r2 & 7) * STEPS + (r2 >> 3))
    perm_back = one_hot(r2 == (t2 & 7) * STEPS + (t2 >> 3))
    p8, g8 = iota((8, ST), 1), iota((8, ST), 0)
    group8 = jnp.where(p8 < LONG, (p8 >> 6) * 2, ((p8 - LONG) >> 5) * 2 + 1)
    spread = one_hot(g8 == group8)
    pace_s[...] = mm(nt(perm, pace_v[...], HI), spread, HI)
    fading_s[...] = mm(nt(perm, fading_v[...], HI), spread, HI)
    lifted_p = mm(perm.astype(BF16), lifted_v[...])
    lifted_s[...] = lifted_p

    def flat(long_ref, short_ref, e):
        a = mm(long_ref[e], one_hot(iota((64, LONG), 0) == (iota((64, LONG), 1) & 63)), HI)
        own = iota((32, LONG), 0) == tp * 4 + (iota((32, LONG), 1) >> 6)
        a = jnp.sum(jnp.where(own, a, 0.0), axis=0, keepdims=True)
        b = mm(short_ref[e], one_hot(iota((32, CH), 0) == (iota((32, CH), 1) & 31)), HI)
        own = iota((32, CH), 0) == tp * 4 + (iota((32, CH), 1) >> 5)
        b = jnp.sum(jnp.where(own, b, 0.0), axis=0, keepdims=True)
        return jnp.concatenate([a, b], axis=1)

    rates = [flat(rate_lv, rate_sv, e) for e in range(2)]
    turns = [flat(turn_lv, turn_sv, e) for e in range(2)]

    tile_l = one_hot(iota((64, LONG), 0) == (iota((64, LONG), 1) & 63))
    tile_s = one_hot(iota((32, CH), 0) == (iota((32, CH), 1) & 31))
    own_l = (iota((64, LONG), 0) >> 4) == (iota((64, LONG), 1) >> 6)
    own_s = (iota((64, CH), 0) >> 4) == (iota((64, CH), 1) >> 5)
    maps_v[...] = jnp.zeros(maps_v.shape, F32)
    for e in range(2):
        for io in range(2):
            for part in range(2):
                a = mm(proj_lv[e, io, part].reshape(64, 64), tile_l, HI)
                a = jnp.where(own_l, a, 0.0)
                b = mm(proj_sv[e, io, part].reshape(64, 32), tile_s, HI)
                b = jnp.where(own_s, b, 0.0)
                for n in range(4):
                    rows = slice(16 * n, 16 * n + 16)
                    maps_v[e, io, part, 32 * n : 32 * n + 16, :LONG] = a[rows]
                    maps_v[e, io, part, 32 * n + 16 : 32 * n + 32, LONG:] = b[rows]
    for e in range(2):
        for part in range(2):
            drive_s[e, part] = mm(lifted_p, maps_v[e, 0, part], HI)

    pl.semaphore_wait(barrier, 31 + NZ - 1)

    def pieces(off):
        xt = (x + off) % NX
        up_src = raising.at[:, pl.ds(pl.multiple_of(xt * 256, 256), 256)]
        up_dst = weights.at[0, z, c, pl.ds(x * 64, 64), :]
        down_src = lowering.at[:, pl.ds(pl.multiple_of(xt * 256, 256), 256)]
        down_dst = weights.at[1, z, c, pl.ds(x * 64, 64), :]
        return xt, up_src, up_dst, down_src, down_dst

    sends = []
    for off in (2, 1, 3):
        xt, up_src, up_dst, down_src, down_dst = pieces(off)
        to = (z * NX + xt, tp)
        sends.append(remote(up_src, up_dst, up_send.at[off], up_recv, to))
        sends.append(remote(down_src, down_dst, down_send.at[off], down_recv, to))
    for copy in sends:
        copy.start()
    _, up_src, up_dst, down_src, down_dst = pieces(0)
    pltpu.make_async_copy(up_src, up_dst, up_recv).start()
    pltpu.make_async_copy(down_src, down_dst, down_recv).start()

    def step(s, carry):
        new = []
        for e in range(2):
            rows = pl.ds(pl.multiple_of((s if e == 0 else STEPS - 1 - s) * 8, 8), 8)
            pre, pim, hre, him = carry[4 * e : 4 * e + 4]
            dt = pace_s[rows, :]
            fade = rates[e] * dt
            mag = jnp.exp(fading_s[rows, :] - fade)
            sn, cs = sincos(turns[e] * dt)
            are, aim = mag * cs, mag * sn
            gain = jnp.sqrt(lost(2.0 * fade))
            bre, bim = drive_s[e, 0, rows, :] * gain, drive_s[e, 1, rows, :] * gain
            pre, pim = are * pre - aim * pim, are * pim + aim * pre
            hre, him = are * hre - aim * him + bre, are * him + aim * hre + bim
            prefix_s[e, 0, rows, :] = pre
            prefix_s[e, 1, rows, :] = pim
            state_s[e, 0, rows, :] = hre
            state_s[e, 1, rows, :] = him
            new += [pre, pim, hre, him]
        return tuple(new)

    one, zero = jnp.ones((8, ST), F32), jnp.zeros((8, ST), F32)
    tops = lax.fori_loop(0, STEPS, step, (one, zero, zero, zero) * 2)

    def composed(first, later):
        fre, fim, bre, bim = first
        nre, nim, are, aim = later
        return (
            nre * fre - nim * fim, nre * fim + nim * fre,
            nre * bre - nim * bim + are, nre * bim + nim * bre + aim,
        )

    unit = (jnp.ones((1, ST), F32),) + (jnp.zeros((1, ST), F32),) * 3
    before = []
    totals = []
    for e in range(2):
        run, rows = unit, [None] * CHUNKS
        for n in range(CHUNKS):
            n = n if e == 0 else CHUNKS - 1 - n
            rows[n] = run
            run = composed(run, tuple(m[n : n + 1] for m in tops[4 * e : 4 * e + 4]))
        before.append(tuple(jnp.concatenate([r[q] for r in rows], axis=0) for q in range(4)))
        totals += list(run)
    own_ends = jnp.concatenate(totals, axis=0)
    ends[...] = own_ends
    cx[x] = own_ends
    for off in (1, 3, 2):
        copy = remote(ends, cx.at[x], cx_send.at[off], cx_recv, (z * NX + (x + off) % NX, tp))
        copy.start()
        sends.append(copy)
    arrival(cx.at[pl.ds(0, NX - 1)], cx_recv)

    def as_map(ref, n, e):
        return tuple(ref[n, 4 * e + q : 4 * e + q + 1, :] for q in range(4))

    row = []
    for e in range(2):
        run = unit
        for n in range(NX) if e == 0 else reversed(range(NX)):
            run = composed(run, as_map(cx, n, e))
        row += list(run)
    row_total = jnp.concatenate(row, axis=0)
    row_ends[...] = row_total
    cz[z] = row_total
    for off in (4, 3, 5, 2, 6, 1, 7):
        copy = remote(
            row_ends, cz.at[z], cz_send.at[off], cz_recv, (((z + off) % NZ) * NX + x, tp)
        )
        copy.start()
        sends.append(copy)

    own_block = pl.ds(pl.multiple_of(inner * TOK, TOK), TOK)

    def plane(off):
        to = (chip + off) % (NX * NY)
        return (z * NX + to // NY, (to % NY) * 2 + block)

    def to_plane(src, dst, send, recv):
        @pl.loop(1, NX * NY)
        def _(off):
            remote(src, dst, send.at[off], recv, plane(off)).start()

        @pl.when(c == block)
        def _():
            pltpu.make_async_copy(src, dst, recv).start()

        @pl.when(c != block)
        def _():
            remote(src, dst, send.at[0], recv, plane(0)).start()

    def plane_sent(src, dst, send, recv):
        @pl.loop(1, NX * NY)
        def _(off):
            remote(src, dst, send.at[off], recv, plane(off)).wait_send()

        @pl.when(c != block)
        def _():
            remote(src, dst, send.at[0], recv, plane(0)).wait_send()

    res_dst = res_v.at[own_block, pl.ds(pl.multiple_of(tp * 256, 256), 256)]
    to_plane(residual, res_dst, res_send, res_recv)

    arrival(weights.at[0, z, c], up_recv)
    arrival(weights.at[1, z, c], down_recv)

    def share(kind, zs, slot):
        ref = weights.at[kind, zs, c]
        copy = remote(ref, ref, sib_send.at[slot], sib_recv.at[kind], (sp, sib))
        copy.start()
        sends.append(copy)

    def ring(ref, way, k):
        to = ((z + (1 if way == 0 else NZ - 1)) % NZ) * NX + x
        copy = remote(ref, ref, ring_send.at[way, k], ring_recv.at[way, k], (to, tp))
        copy.start()
        sends.append(copy)

    def kind_of(way, k):
        return k % 2 if way == 0 else 1 - k % 2

    for k in range(2):
        for way in range(2):
            ring(weights.at[kind_of(way, k), z, c], way, k)
    for kind in range(2):
        share(kind, z, kind)

    def ring_step(k):
        for way in range(2):
            hops = k // 2 + 1
            zs = (z + (NZ - hops if way == 0 else hops)) % NZ
            kind = kind_of(way, k)
            ref = weights.at[kind, zs, c]
            arrival(ref, ring_recv.at[way, k])
            if k < 5:
                ring(ref, way, k + 2)
            share(kind, zs, 2 + 2 * k + way)

    arrival(cz.at[pl.ds(0, NZ - 1)], cz_recv)

    def applied(m, state):
        pre, pim, hre, him = m
        re, im = state
        return pre * re - pim * im + hre, pre * im + pim * re + him

    blank = jnp.zeros((1, ST), F32)
    out_y = jnp.zeros((TOK, CH), F32)
    for e in range(2):
        state = (blank, blank)
        for ref, count, at in ((cz, NZ, z), (cx, NX, x)):
            for n in range(count) if e == 0 else reversed(range(count)):
                passed = (n < at) if e == 0 else (n > at)
                new = applied(as_map(ref, n, e), state)
                state = tuple(jnp.where(passed, a, b) for a, b in zip(new, state))
        entry = applied(before[e], state)
        tall = tuple(jnp.concatenate([v] * STEPS, axis=0) for v in entry)
        pre, pim = prefix_s[e, 0], prefix_s[e, 1]
        re = state_s[e, 0] + pre * tall[0] - pim * tall[1]
        im = state_s[e, 1] + pre * tall[1] + pim * tall[0]
        out_y = out_y + nt(re, maps_v[e, 1, 0], HI) - nt(im, maps_v[e, 1, 1], HI)

    mine = iota((8, CH), 0) == tp
    skip_row = jnp.sum(jnp.where(mine, skip_v[...], 0.0), axis=0, keepdims=True)
    closing_row = jnp.sum(jnp.where(mine, closing_v[...], 0.0), axis=0, keepdims=True)
    v = out_y + skip_row * lifted_s[...]
    act = 0.5 * v * (1.0 + jnp.tanh(0.7978845608028654 * (v + 0.044715 * v * v * v)))
    act = act * lax.rsqrt(jnp.mean(act * act, axis=1, keepdims=True) + EPSILON) * closing_row
    merged_v[...] = mm(perm_back.astype(BF16), act.astype(BF16)).astype(BF16)
    mg_dst = gathered.at[own_block, pl.ds(pl.multiple_of(tp * CH, CH), CH)]
    to_plane(merged_v, mg_dst, mg_send, mg_recv)

    for k in range(4):
        ring_step(k)
    copies[-1].wait()
    arrival(res_v, res_recv)
    arrival(gathered, mg_recv)

    def project(n, squares):
        cols = pl.ds(pl.multiple_of(n * 256, 256), 256)
        m = mm(gathered[...], emitted_v[:, cols]) + res_v[:, cols].astype(F32)
        mid_f[:, cols] = m
        mid_v[:, cols] = (m * leading_v[:, cols]).astype(BF16)
        return squares + jnp.sum(m * m, axis=1, keepdims=True)

    squares = lax.fori_loop(0, 8, project, jnp.zeros((2 * TOK, 1), F32))
    scale = lax.rsqrt(squares * (1.0 / D) + EPSILON)

    own_cols = pl.ds(pl.multiple_of(tp * 256, 256), 256)
    sib_cols = pl.ds(pl.multiple_of(sib * 256, 256), 256)

    @pl.when(c == block)
    def _():
        remote(mid_f.at[own_block, sib_cols], own_mid, mid_send, mid_recv, (sp, sib)).start()

    for k in range(4, 7):
        ring_step(k)

    arrival(weights.at[0, :, 1 - c], sib_recv.at[0])
    for n in range(2):
        up = mm(mid_v[...], weights[0, :, n].reshape(D, 256)) * scale
        up = jnp.maximum(up, 0.0)
        hidden[:, n * 256 : (n + 1) * 256] = (up * up).astype(BF16)
    arrival(weights.at[1, :, 1 - c], sib_recv.at[1])

    def down(n):
        both = nt(hidden[:, :256], weights[1, n, 0]) + nt(hidden[:, 256:], weights[1, n, 1])
        partial[n] = both.astype(BF16)

    def part(n, i):
        return remote(
            partial.at[n, pl.ds(i * TOK, TOK), :], arrived.at[chip],
            rs_send.at[n, i], rs_recv, (z * NX + 2 * c + i, n),
        )

    @pl.loop(1, 8)
    def _(off):
        n = (tp + off) % 8
        down(n)
        for i in range(2):
            part(n, i).start()

    down(tp)
    for i in range(2):
        here = (2 * c + i) == x

        @pl.when(here)
        def _():
            pltpu.make_async_copy(
                partial.at[tp, pl.ds(i * TOK, TOK), :], arrived.at[chip], rs_recv
            ).start()

        @pl.when(jnp.logical_not(here))
        def _():
            part(tp, i).start()

    @pl.when(c == block)
    def _():
        own_mid_copy = pltpu.make_async_copy(mid_f.at[own_block, own_cols], own_mid, mid_recv)
        own_mid_copy.start()

    arrival(own_mid, mid_recv)
    arrival(arrived, rs_recv)
    total = own_mid[...]
    for n in range(NX * NY):
        total = total + arrived[n].astype(F32)
    out[...] = total.astype(BF16)

    for copy in sends:
        copy.wait_send()
    plane_sent(residual, res_dst, res_send, res_recv)
    plane_sent(merged_v, mg_dst, mg_send, mg_recv)

    @pl.when(c == block)
    def _():
        remote(mid_f.at[own_block, sib_cols], own_mid, mid_send, mid_recv, (sp, sib)).wait_send()

    @pl.loop(1, 8)
    def _(off):
        for i in range(2):
            part((tp + off) % 8, i).wait_send()

    for i in range(2):

        @pl.when((2 * c + i) != x)
        def _():
            part(tp, i).wait_send()


def on_device(
    residual, lifted, pace, fading, rate_l, rate_s, turn_l, turn_s, proj_l, proj_s,
    skip, closing, emitted, leading, raising, lowering,
):
    dma = pltpu.SemaphoreType.DMA
    vm = pltpu.VMEM
    return pl.pallas_call(
        kernel,
        out_shape=jax.ShapeDtypeStruct((TOK, 256), BF16),
        in_specs=[pl.BlockSpec(memory_space=pl.ANY)] * 16,
        out_specs=pl.BlockSpec(memory_space=pltpu.VMEM),
        scratch_shapes=[
            vm((TOK, CH), BF16), vm((8, TOK), F32), vm((8, TOK), F32),
            vm((2, 32, 64), F32), vm((2, 32, 32), F32), vm((2, 32, 64), F32), vm((2, 32, 32), F32),
            vm((2, 2, 2, 4, 16, 64), F32), vm((2, 2, 2, 4, 16, 32), F32),
            vm((8, CH), F32), vm((8, CH), F32), vm((1024, D), BF16), vm((1, D), F32),
            vm((2, 2, 2, CH, ST), F32), vm((TOK, ST), F32), vm((TOK, ST), F32),
            vm((2, 2, TOK, ST), F32), vm((2, 2, TOK, ST), F32), vm((2, 2, TOK, ST), F32),
            vm((TOK, CH), F32),
            vm((8, ST), F32), vm((NX, 8, ST), F32), vm((NZ, 8, ST), F32), vm((8, ST), F32),
            vm((TOK, CH), BF16), vm((2 * TOK, 1024), BF16), vm((2 * TOK, D), BF16),
            vm((2 * TOK, D), BF16), vm((2 * TOK, D), F32), vm((TOK, 256), F32),
            vm((2, NZ, 2, 256, 256), BF16), vm((2 * TOK, 512), BF16),
            vm((8, 2 * TOK, 256), BF16), vm((NX * NY, TOK, 256), BF16),
            dma((13,)), dma((NX,)), dma, dma((NX,)), dma, dma((NX,)), dma, dma((NZ,)), dma,
            dma((16,)), dma, dma((8, 2)), dma, dma((16,)), dma, dma((2, 7)), dma((2, 7)),
            dma((16,)), dma((2,)), dma, dma,
        ],
        compiler_params=pltpu.CompilerParams(
            collective_id=0, has_side_effects=True, vmem_limit_bytes=60 * 1024 * 1024
        ),
        name="layer",
    )(
        residual, lifted, pace, fading, rate_l, rate_s, turn_l, turn_s,
        proj_l.swapaxes(-1, -2), proj_s.swapaxes(-1, -2),
        skip.reshape(8, CH), closing.reshape(8, CH), emitted, leading.reshape(1, D), raising, lowering.T,
    )


def solution(mesh):
    rest = [P()] * 10
    return jax.shard_map(
        on_device,
        mesh=mesh,
        in_specs=(P("sp", "tp"), P("sp", "tp"), P("tp", "sp"), P("tp", "sp"), *rest, P("sp", "tp"), P("tp", "sp")),
        out_specs=P("sp", "tp"),
        check_vma=False,
    )
```

time: 205 us -> 66.7 us (0.33)
  blocking collectives: 81.8 us -> 0 us
  Pallas kernels: 0 us -> 65.1 us
  local copies, waits for them, and re-layouts: 49.7 us -> 1.47 us
  other arithmetic: 21.6 us -> 0 us
  between operations: 16.8 us -> 0.01 us
  starting transfers between devices: 16.2 us -> 0 us
  matrix products: 13.2 us -> 0 us
  waiting for transfers between devices: 3.81 us -> 0 us
    pallas_call x0 -> x1, Pallas kernels: none -> 65.1 us  [on_device(): pl.pallas_call(kernel, out_shape=jax.ShapeDtypeStruct((TOK, 256), BF16),...]
    all_to_all x4 -> x0, blocking collectives: 50.1 us -> none  [the longest x1 16.9 us: on_device(): lax.all_to_all(combined_result, 'tp', split_axis=0, concat_axis=1, tiled=...]
    slice x243 -> x0, local copies, waits for them, and re-layouts: 34.2 us -> none  [the longest x196 29.8 us: scanned(): return lax.associative_scan(combine_maps, maps, reverse=backward, axis=0)]
    all_gather x2 -> x0, blocking collectives: 31.8 us -> none  [gathered_once(): both, at, found = (lax.all_gather(jnp.concatenate(lines), axis), 0, {})]
    all_to_all x2 -> x0, starting transfers between devices: 16 us -> none  [sent_to_all(): return lax.all_to_all(copies, axis, split_axis=0, concat_axis=0, tiled=True)]
    dot_general x10 -> x0, matrix products: 13.2 us -> none  [the longest x1 5.59 us: on_device(): jnp.dot(hidden, down_whole, preferred_element_type=jnp.float32)]
    add x101 -> x0, other arithmetic: 8.61 us -> none  [the longest x27 5.69 us: combine_maps(): next_re * base_im + next_im * base_re + add_im]
    concatenate x52 -> x0, other arithmetic: 6.81 us -> none  [the longest x48 6.03 us: scanned(): return lax.associative_scan(combine_maps, maps, reverse=backward, axis=0)]
  transfers between devices with their start and end apart: 3 -> 0, of which waited for: 1 -> 0; matrix products, arithmetic and copies ran while one was open for 32% -> 0% of each run, Pallas kernels for 0% -> 0%
where the time goes in v1:
time: 66.7 us; the launch traced here: 66.6 us
  Pallas kernels  65.1 us (98%)
  local copies, waits for them, and re-layouts  1.47 us (2%)
    pallas_call x1, Pallas kernels, on_device(): pl.pallas_call(kernel, out_shape=jax.ShapeDtypeStruct((TOK, 256), BF16),...  65.1 us
    unnamed x1, local copies, waits for them, and re-layouts  1.47 us

profile of v1, /device:TPU:1, one launch (start us, length us, event | category | flops | bytes accessed | tf_op | source)
XLA Modules:
  0.0 66.6 jit_solution(18254766467083453063)
XLA Ops:
  0.0 65.1 %layer.1 = bf16[128,256]{1,0:T(8,128)(2,1)} custom-call(bf16[128,256]{1,0:T(8,128)(2,1)} %residual.1, bf16[128,128]{1,0:T(8,128)(2,1)} %lifted.1, f32[8,128]{1,0:T(8,128)} %pace.1, f32[8,128]{1,0:T(8,128)} %fading.1, f32[2,32,64]{2,1,0:T(8,128)} %rate_l.1, f32[2,32,32]{2,1,0:T(8,128)} %rate_s.1, f32[2,32,64]{2,1,0:T(8,128)} %turn_l.1, f32[2,32,32]{2,1,0:T(8,128)} %turn_s.1, ...), custom_call_target="tpu_custom_call" | custom-call | tf_op jit(solution)/shard_map/layer/pallas_call | solution.py:460
  65.1 1.5 %copy.18 = bf16[128,256]{1,0:T(8,128)(2,1)} copy(bf16[128,256]{1,0:T(8,128)(2,1)} %layer.1) | data formatting | bytes 131072

commit v2 on v1

--- a/solution.py
+++ b/solution.py
@@ -37,6 +37,11 @@
 
 def mm(a, b, precision=None):
     return jnp.dot(a, b, precision=precision, preferred_element_type=F32)
+
+
+def halves(a):
+    high = a.astype(BF16)
+    return high, (a - high.astype(F32)).astype(BF16)
 
 
 def sincos(a):
@@ -66,12 +71,12 @@
     skip, closing, emitted, leading, raising, lowering,
     out,
     lifted_v, pace_v, fading_v, rate_lv, rate_sv, turn_lv, turn_sv, proj_lv, proj_sv,
-    skip_v, closing_v, emitted_v, leading_v,
+    skip_v, closing_v, raising_v, lowering_v, emitted_v, leading_v,
     maps_v, pace_s, fading_s, drive_s, prefix_s, state_s, lifted_s,
     ends, cx, cz, row_ends, merged_v, gathered, res_v, mid_v, mid_f, own_mid,
-    weights, hidden, partial, arrived,
+    weights, hidden, partial, from_y, from_x, sum_y, sum_x, final,
     load_sem, up_send, up_recv, down_send, down_recv, cx_send, cx_recv, cz_send, cz_recv,
-    mg_send, mg_recv, rs_send, rs_recv, res_send, res_recv, ring_send, ring_recv,
+    mg_send, mg_recv, ay_send, ay_recv, ax_send, ax_recv, fy_send, fx_send, final_recv, res_send, res_recv, ring_send, ring_recv,
     sib_send, sib_recv, mid_send, mid_recv,
 ):
     sp = lax.axis_index("sp")
@@ -111,12 +116,13 @@
         (rate_s, rate_sv), (turn_l, turn_lv), (turn_s, turn_sv),
         (proj_l.at[:, :, :, pl.ds(tp * 4, 4)], proj_lv),
         (proj_s.at[:, :, :, pl.ds(tp * 4, 4)], proj_sv),
-        (skip, skip_v), (closing, closing_v), (leading, leading_v), (emitted, emitted_v),
+        (skip, skip_v), (closing, closing_v), (raising, raising_v), (lowering, lowering_v),
+        (leading, leading_v), (emitted, emitted_v),
     ]
     copies = [pltpu.make_async_copy(a, b, load_sem.at[n]) for n, (a, b) in enumerate(loads)]
     for copy in copies:
         copy.start()
-    for copy in copies[:-1]:
+    for copy in copies[:-4]:
         copy.wait()
 
     r2, t2 = iota((TOK, TOK), 0), iota((TOK, TOK), 1)
@@ -142,44 +148,52 @@
     rates = [flat(rate_lv, rate_sv, e) for e in range(2)]
     turns = [flat(turn_lv, turn_sv, e) for e in range(2)]
 
-    tile_l = one_hot(iota((64, LONG), 0) == (iota((64, LONG), 1) & 63))
-    tile_s = one_hot(iota((32, CH), 0) == (iota((32, CH), 1) & 31))
+    tile_l = one_hot(iota((64, LONG), 0) == (iota((64, LONG), 1) & 63)).astype(BF16)
+    tile_s = one_hot(iota((32, CH), 0) == (iota((32, CH), 1) & 31)).astype(BF16)
     own_l = (iota((64, LONG), 0) >> 4) == (iota((64, LONG), 1) >> 6)
     own_s = (iota((64, CH), 0) >> 4) == (iota((64, CH), 1) >> 5)
-    maps_v[...] = jnp.zeros(maps_v.shape, F32)
+    maps_v[...] = jnp.zeros(maps_v.shape, BF16)
     for e in range(2):
         for io in range(2):
             for part in range(2):
-                a = mm(proj_lv[e, io, part].reshape(64, 64), tile_l, HI)
-                a = jnp.where(own_l, a, 0.0)
-                b = mm(proj_sv[e, io, part].reshape(64, 32), tile_s, HI)
-                b = jnp.where(own_s, b, 0.0)
-                for n in range(4):
-                    rows = slice(16 * n, 16 * n + 16)
-                    maps_v[e, io, part, 32 * n : 32 * n + 16, :LONG] = a[rows]
-                    maps_v[e, io, part, 32 * n + 16 : 32 * n + 32, LONG:] = b[rows]
+                wide = halves(proj_lv[e, io, part].reshape(64, 64))
+                slim = halves(proj_sv[e, io, part].reshape(64, 32))
+                for h in range(2):
+                    a = jnp.where(own_l, mm(wide[h], tile_l), 0.0).astype(BF16)
+                    b = jnp.where(own_s, mm(slim[h], tile_s), 0.0).astype(BF16)
+                    for n in range(4):
+                        rows = slice(16 * n, 16 * n + 16)
+                        maps_v[e, io, part, h, 32 * n : 32 * n + 16, :LONG] = a[rows]
+                        maps_v[e, io, part, h, 32 * n + 16 : 32 * n + 32, LONG:] = b[rows]
+    lifted_b = lifted_p.astype(BF16)
     for e in range(2):
         for part in range(2):
-            drive_s[e, part] = mm(lifted_p, maps_v[e, 0, part], HI)
-
+            drive_s[e, part] = mm(lifted_b, maps_v[e, 0, part, 0]) + mm(lifted_b, maps_v[e, 0, part, 1])
+
+    copies[-4].wait()
+    copies[-3].wait()
     pl.semaphore_wait(barrier, 31 + NZ - 1)
+
+    sends = []
+
+    def begin(copy):
+        copy.start()
+        sends.append(copy)
 
     def pieces(off):
         xt = (x + off) % NX
-        up_src = raising.at[:, pl.ds(pl.multiple_of(xt * 256, 256), 256)]
+        up_src = raising_v.at[:, pl.ds(pl.multiple_of(xt * 256, 256), 256)]
         up_dst = weights.at[0, z, c, pl.ds(x * 64, 64), :]
-        down_src = lowering.at[:, pl.ds(pl.multiple_of(xt * 256, 256), 256)]
+        down_src = lowering_v.at[:, pl.ds(pl.multiple_of(xt * 256, 256), 256)]
         down_dst = weights.at[1, z, c, pl.ds(x * 64, 64), :]
         return xt, up_src, up_dst, down_src, down_dst
 
-    sends = []
     for off in (2, 1, 3):
-        xt, up_src, up_dst, down_src, down_dst = pieces(off)
-        to = (z * NX + xt, tp)
-        sends.append(remote(up_src, up_dst, up_send.at[off], up_recv, to))
-        sends.append(remote(down_src, down_dst, down_send.at[off], down_recv, to))
-    for copy in sends:
-        copy.start()
+        xt, src, dst, _, _ = pieces(off)
+        begin(remote(src, dst, up_send.at[off], up_recv, (z * NX + xt, tp)))
+    for off in (2, 1, 3):
+        xt, _, _, src, dst = pieces(off)
+        begin(remote(src, dst, down_send.at[off], down_recv, (z * NX + xt, tp)))
     _, up_src, up_dst, down_src, down_dst = pieces(0)
     pltpu.make_async_copy(up_src, up_dst, up_recv).start()
     pltpu.make_async_copy(down_src, down_dst, down_recv).start()
@@ -230,10 +244,70 @@
     own_ends = jnp.concatenate(totals, axis=0)
     ends[...] = own_ends
     cx[x] = own_ends
-    for off in (1, 3, 2):
+
+    for off in (2, 1, 3):
         copy = remote(ends, cx.at[x], cx_send.at[off], cx_recv, (z * NX + (x + off) % NX, tp))
         copy.start()
         sends.append(copy)
+    ORDER = (
+        (0, 0, 0), (0, 1, 0), (1, 0, 0), (0, 0, 1), (0, 1, 1), (1, 1, 0), (0, 0, 2),
+        (0, 1, 2), (1, 0, 1), (0, 0, 3), (1, 1, 1), (1, 0, 2), (1, 1, 2), (1, 0, 3),
+    )
+
+    def piece(way, slot, extra):
+        kind, half, hops = ORDER[slot]
+        hops = hops + extra
+        zs = (z + (NZ - hops if way == 0 else hops)) % NZ
+        return kind, weights.at[kind, zs, c, pl.ds((half ^ way) * 128, 128), :]
+
+    def share(kind, ref, slot):
+        begin(remote(ref, ref, sib_send.at[slot], sib_recv.at[kind], (sp, sib)))
+
+    def ring_send_slot(slot):
+        for way in range(2):
+            to = ((z + (1 if way == 0 else NZ - 1)) % NZ) * NX + x
+            _, ref = piece(way, slot, 0)
+            begin(remote(ref, ref, ring_send.at[way, slot], ring_recv.at[way, slot], (to, tp)))
+
+    def ring_take(slot):
+        for way in range(2):
+            kind, ref = piece(way, slot, 1)
+            arrival(ref, ring_recv.at[way, slot])
+            share(kind, ref, 2 + 2 * slot + way)
+
+    own_block = pl.ds(pl.multiple_of(inner * TOK, TOK), TOK)
+
+    def plane(off):
+        to = (chip + off) % (NX * NY)
+        return (z * NX + to // NY, (to % NY) * 2 + block)
+
+    def to_plane(src, dst, send, recv):
+        @pl.loop(1, NX * NY)
+        def _(off):
+            remote(src, dst, send.at[off], recv, plane(off)).start()
+
+        @pl.when(c == block)
+        def _():
+            pltpu.make_async_copy(src, dst, recv).start()
+
+        @pl.when(c != block)
+        def _():
+            remote(src, dst, send.at[0], recv, plane(0)).start()
+
+    def plane_sent(src, dst, send, recv):
+        @pl.loop(1, NX * NY)
+        def _(off):
+            remote(src, dst, send.at[off], recv, plane(off)).wait_send()
+
+        @pl.when(c != block)
+        def _():
+            remote(src, dst, send.at[0], recv, plane(0)).wait_send()
+
+    res_dst = res_v.at[own_block, pl.ds(pl.multiple_of(tp * 256, 256), 256)]
+    arrival(weights.at[0, z, c], up_recv)
+    ring_send_slot(0)
+    ring_send_slot(1)
+    share(0, weights.at[0, z, c], 0)
     arrival(cx.at[pl.ds(0, NX - 1)], cx_recv)
 
     def as_map(ref, n, e):
@@ -255,71 +329,16 @@
         copy.start()
         sends.append(copy)
 
-    own_block = pl.ds(pl.multiple_of(inner * TOK, TOK), TOK)
-
-    def plane(off):
-        to = (chip + off) % (NX * NY)
-        return (z * NX + to // NY, (to % NY) * 2 + block)
-
-    def to_plane(src, dst, send, recv):
-        @pl.loop(1, NX * NY)
-        def _(off):
-            remote(src, dst, send.at[off], recv, plane(off)).start()
-
-        @pl.when(c == block)
-        def _():
-            pltpu.make_async_copy(src, dst, recv).start()
-
-        @pl.when(c != block)
-        def _():
-            remote(src, dst, send.at[0], recv, plane(0)).start()
-
-    def plane_sent(src, dst, send, recv):
-        @pl.loop(1, NX * NY)
-        def _(off):
-            remote(src, dst, send.at[off], recv, plane(off)).wait_send()
-
-        @pl.when(c != block)
-        def _():
-            remote(src, dst, send.at[0], recv, plane(0)).wait_send()
-
-    res_dst = res_v.at[own_block, pl.ds(pl.multiple_of(tp * 256, 256), 256)]
+    arrival(weights.at[1, z, c], down_recv)
+    ring_send_slot(2)
+    share(1, weights.at[1, z, c], 1)
     to_plane(residual, res_dst, res_send, res_recv)
 
-    arrival(weights.at[0, z, c], up_recv)
-    arrival(weights.at[1, z, c], down_recv)
-
-    def share(kind, zs, slot):
-        ref = weights.at[kind, zs, c]
-        copy = remote(ref, ref, sib_send.at[slot], sib_recv.at[kind], (sp, sib))
-        copy.start()
-        sends.append(copy)
-
-    def ring(ref, way, k):
-        to = ((z + (1 if way == 0 else NZ - 1)) % NZ) * NX + x
-        copy = remote(ref, ref, ring_send.at[way, k], ring_recv.at[way, k], (to, tp))
-        copy.start()
-        sends.append(copy)
-
-    def kind_of(way, k):
-        return k % 2 if way == 0 else 1 - k % 2
-
-    for k in range(2):
-        for way in range(2):
-            ring(weights.at[kind_of(way, k), z, c], way, k)
-    for kind in range(2):
-        share(kind, z, kind)
-
-    def ring_step(k):
-        for way in range(2):
-            hops = k // 2 + 1
-            zs = (z + (NZ - hops if way == 0 else hops)) % NZ
-            kind = kind_of(way, k)
-            ref = weights.at[kind, zs, c]
-            arrival(ref, ring_recv.at[way, k])
-            if k < 5:
-                ring(ref, way, k + 2)
-            share(kind, zs, 2 + 2 * k + way)
+    ring_take(0)
+    ring_send_slot(3)
+    ring_take(1)
+    ring_send_slot(4)
+    ring_send_slot(5)
 
     arrival(cz.at[pl.ds(0, NZ - 1)], cz_recv)
 
@@ -342,7 +361,10 @@
         pre, pim = prefix_s[e, 0], prefix_s[e, 1]
         re = state_s[e, 0] + pre * tall[0] - pim * tall[1]
         im = state_s[e, 1] + pre * tall[1] + pim * tall[0]
-        out_y = out_y + nt(re, maps_v[e, 1, 0], HI) - nt(im, maps_v[e, 1, 1], HI)
+        for part, value in ((0, re), (1, -im)):
+            high, low = halves(value)
+            out_y = out_y + nt(high, maps_v[e, 1, part, 0])
+            out_y = out_y + (nt(low, maps_v[e, 1, part, 0]) + nt(high, maps_v[e, 1, part, 1]))
 
     mine = iota((8, CH), 0) == tp
     skip_row = jnp.sum(jnp.where(mine, skip_v[...], 0.0), axis=0, keepdims=True)
@@ -354,20 +376,40 @@
     mg_dst = gathered.at[own_block, pl.ds(pl.multiple_of(tp * CH, CH), CH)]
     to_plane(merged_v, mg_dst, mg_send, mg_recv)
 
-    for k in range(4):
-        ring_step(k)
+    ring_take(2)
+    ring_take(3)
+    ring_send_slot(6)
+    ring_take(4)
+    ring_send_slot(7)
+    ring_send_slot(8)
+    ring_take(5)
+    ring_take(6)
+    ring_send_slot(9)
+    ring_send_slot(10)
+    ring_take(7)
+    ring_take(8)
+    ring_send_slot(11)
+    ring_take(9)
+    ring_take(10)
+    ring_send_slot(12)
+    ring_take(11)
+    ring_send_slot(13)
     copies[-1].wait()
+    copies[-2].wait()
     arrival(res_v, res_recv)
+    ring_take(12)
     arrival(gathered, mg_recv)
 
     def project(n, squares):
-        cols = pl.ds(pl.multiple_of(n * 256, 256), 256)
+        cols = pl.ds(pl.multiple_of(n * 512, 512), 512)
         m = mm(gathered[...], emitted_v[:, cols]) + res_v[:, cols].astype(F32)
         mid_f[:, cols] = m
         mid_v[:, cols] = (m * leading_v[:, cols]).astype(BF16)
         return squares + jnp.sum(m * m, axis=1, keepdims=True)
 
-    squares = lax.fori_loop(0, 8, project, jnp.zeros((2 * TOK, 1), F32))
+    squares = lax.fori_loop(0, 2, project, jnp.zeros((2 * TOK, 1), F32))
+    ring_take(13)
+    squares = lax.fori_loop(2, 4, project, squares)
     scale = lax.rsqrt(squares * (1.0 / D) + EPSILON)
 
     own_cols = pl.ds(pl.multiple_of(tp * 256, 256), 256)
@@ -376,9 +418,6 @@
     @pl.when(c == block)
     def _():
         remote(mid_f.at[own_block, sib_cols], own_mid, mid_send, mid_recv, (sp, sib)).start()
-
-    for k in range(4, 7):
-        ring_step(k)
 
     arrival(weights.at[0, :, 1 - c], sib_recv.at[0])
     for n in range(2):
@@ -391,44 +430,103 @@
         both = nt(hidden[:, :256], weights[1, n, 0]) + nt(hidden[:, 256:], weights[1, n, 1])
         partial[n] = both.astype(BF16)
 
-    def part(n, i):
-        return remote(
-            partial.at[n, pl.ds(i * TOK, TOK), :], arrived.at[chip],
-            rs_send.at[n, i], rs_recv, (z * NX + 2 * c + i, n),
-        )
-
-    @pl.loop(1, 8)
-    def _(off):
-        n = (tp + off) % 8
-        down(n)
+    def row_of(k):
+        return (y + 1 + k) % NY
+
+    def along_y(i, k):
+        to = row_of(k)
+        src = partial.at[2 * to + 1, pl.ds(i * TOK, TOK), :]
+        dst = from_y.at[i, y]
+        return src, dst, remote(src, dst, ay_send.at[i, k], ay_recv.at[i], (sp, 2 * to + c))
+
+    def along_x(k, i):
+        src = partial.at[2 * row_of(k), pl.ds(i * TOK, TOK), :]
+        dst = from_x.at[row_of(k), x]
+        to = (z * NX + 2 * c + i, tp)
+        return src, dst, remote(src, dst, ax_send.at[k, i], ax_recv.at[k], to)
+
+    def on_y(i):
+        dst = final.at[x]
+        to = (z * NX + 2 * c + i, y * 2 + 1)
+        return sum_y.at[i], dst, remote(sum_y.at[i], dst, fy_send.at[i], final_recv, to)
+
+    def on_x(k):
+        dst = final.at[y]
+        to = (sp, row_of(k) * 2)
+        return sum_x.at[k], dst, remote(sum_x.at[k], dst, fx_send.at[k], final_recv, to)
+
+    def deliver(triple, recv, local):
+        src, dst, copy = triple
+        if local is None:
+            copy.start()
+            return
+
+        @pl.when(local)
+        def _():
+            pltpu.make_async_copy(src, dst, recv).start()
+
+        @pl.when(jnp.logical_not(local))
+        def _():
+            copy.start()
+
+    def delivered(triple, local):
+        if local is None:
+            triple[2].wait_send()
+            return
+
+        @pl.when(jnp.logical_not(local))
+        def _():
+            triple[2].wait_send()
+
+    def near(i):
+        return (2 * c + i) == x
+
+    def local_y(k):
+        return (c == 0) if k == NY - 1 else None
+
+    for k in range(NY):
+        down(2 * row_of(k) + 1)
+        if k < NY - 1:
+            along_y(0, k)[2].start()
+        else:
+            for i in range(2):
+                src, dst, _ = along_y(i, k)
+                pltpu.make_async_copy(src, dst, ay_recv.at[i]).start()
+        down(2 * row_of(k))
         for i in range(2):
-            part(n, i).start()
-
-    down(tp)
-    for i in range(2):
-        here = (2 * c + i) == x
-
-        @pl.when(here)
-        def _():
-            pltpu.make_async_copy(
-                partial.at[tp, pl.ds(i * TOK, TOK), :], arrived.at[chip], rs_recv
-            ).start()
-
-        @pl.when(jnp.logical_not(here))
-        def _():
-            part(tp, i).start()
+            deliver(along_x(k, i), ax_recv.at[k], near(i))
+    for k in range(NY - 1):
+        along_y(1, k)[2].start()
+
+    def summed(ref):
+        total = ref[0].astype(F32)
+        for n in range(1, NX):
+            total = total + ref[n].astype(F32)
+        return total
+
+    def turn_x(k):
+        @pl.when(c == block)
+        def _():
+            arrival(from_x.at[row_of(k)], ax_recv.at[k])
+            sum_x[k] = summed(from_x.at[row_of(k)]).astype(BF16)
+            deliver(on_x(k), final_recv, local_y(k))
+
+    def turn_y(i):
+        arrival(from_y.at[i], ay_recv.at[i])
+        sum_y[i] = summed(from_y.at[i]).astype(BF16)
+        deliver(on_y(i), final_recv, jnp.logical_and(near(i), c == 1))
 
     @pl.when(c == block)
     def _():
         own_mid_copy = pltpu.make_async_copy(mid_f.at[own_block, own_cols], own_mid, mid_recv)
         own_mid_copy.start()
 
-    arrival(own_mid, mid_recv)
-    arrival(arrived, rs_recv)
-    total = own_mid[...]
-    for n in range(NX * NY):
-        total = total + arrived[n].astype(F32)
-    out[...] = total.astype(BF16)
+    turn_x(0)
+    turn_y(0)
+    turn_x(1)
+    turn_x(2)
+    turn_x(3)
+    turn_y(1)
 
     for copy in sends:
         copy.wait_send()
@@ -439,16 +537,22 @@
     def _():
         remote(mid_f.at[own_block, sib_cols], own_mid, mid_send, mid_recv, (sp, sib)).wait_send()
 
-    @pl.loop(1, 8)
-    def _(off):
+    arrival(own_mid, mid_recv)
+    arrival(final, final_recv)
+    out[...] = (own_mid[...] + summed(final)).astype(BF16)
+
+    for k in range(NY):
         for i in range(2):
-            part((tp + off) % 8, i).wait_send()
+            delivered(along_x(k, i), near(i))
+            if k < NY - 1:
+                along_y(i, k)[2].wait_send()
+
+        @pl.when(c == block)
+        def _():
+            delivered(on_x(k), local_y(k))
 
     for i in range(2):
-
-        @pl.when((2 * c + i) != x)
-        def _():
-            part(tp, i).wait_send()
+        delivered(on_y(i), jnp.logical_and(near(i), c == 1))
 
 
 def on_device(
@@ -466,18 +570,19 @@
             vm((TOK, CH), BF16), vm((8, TOK), F32), vm((8, TOK), F32),
             vm((2, 32, 64), F32), vm((2, 32, 32), F32), vm((2, 32, 64), F32), vm((2, 32, 32), F32),
             vm((2, 2, 2, 4, 16, 64), F32), vm((2, 2, 2, 4, 16, 32), F32),
-            vm((8, CH), F32), vm((8, CH), F32), vm((1024, D), BF16), vm((1, D), F32),
-            vm((2, 2, 2, CH, ST), F32), vm((TOK, ST), F32), vm((TOK, ST), F32),
+            vm((8, CH), F32), vm((8, CH), F32), vm((64, 1024), BF16), vm((64, 1024), BF16), vm((1024, D), BF16), vm((1, D), F32),
+            vm((2, 2, 2, 2, CH, ST), BF16), vm((TOK, ST), F32), vm((TOK, ST), F32),
             vm((2, 2, TOK, ST), F32), vm((2, 2, TOK, ST), F32), vm((2, 2, TOK, ST), F32),
             vm((TOK, CH), F32),
             vm((8, ST), F32), vm((NX, 8, ST), F32), vm((NZ, 8, ST), F32), vm((8, ST), F32),
             vm((TOK, CH), BF16), vm((2 * TOK, 1024), BF16), vm((2 * TOK, D), BF16),
             vm((2 * TOK, D), BF16), vm((2 * TOK, D), F32), vm((TOK, 256), F32),
             vm((2, NZ, 2, 256, 256), BF16), vm((2 * TOK, 512), BF16),
-            vm((8, 2 * TOK, 256), BF16), vm((NX * NY, TOK, 256), BF16),
-            dma((13,)), dma((NX,)), dma, dma((NX,)), dma, dma((NX,)), dma, dma((NZ,)), dma,
-            dma((16,)), dma, dma((8, 2)), dma, dma((16,)), dma, dma((2, 7)), dma((2, 7)),
-            dma((16,)), dma((2,)), dma, dma,
+            vm((8, 2 * TOK, 256), BF16), vm((2, NY, TOK, 256), BF16), vm((NY, NX, TOK, 256), BF16),
+            vm((2, TOK, 256), BF16), vm((NY, TOK, 256), BF16), vm((4, TOK, 256), BF16),
+            dma((15,)), dma((NX,)), dma, dma((NX,)), dma, dma((NX,)), dma, dma((NZ,)), dma,
+            dma((16,)), dma, dma((2, 4)), dma((2,)), dma((4, 2)), dma((4,)), dma((2,)), dma((4,)), dma, dma((16,)), dma, dma((2, 14)), dma((2, 14)),
+            dma((30,)), dma((2,)), dma, dma,
         ],
         compiler_params=pltpu.CompilerParams(
             collective_id=0, has_side_effects=True, vmem_limit_bytes=60 * 1024 * 1024

time: 66.7 us -> 59.1 us (0.89)
  the two profiles are of different devices: /device:TPU:1 before, /device:TPU:3 now
where the time goes in v2:
time: 59.1 us; the launch traced here: 58.9 us
  Pallas kernels  57.5 us (97%)
  local copies, waits for them, and re-layouts  1.47 us (2%)
    pallas_call x1, Pallas kernels, on_device(): pl.pallas_call(kernel, out_shape=jax.ShapeDtypeStruct((TOK, 256), BF16),...  57.5 us
    unnamed x1, local copies, waits for them, and re-layouts  1.47 us

profile of v2, /device:TPU:3, one launch (start us, length us, event | category | flops | bytes accessed | tf_op | source)
XLA Modules:
  0.0 58.9 jit_solution(10928432446013863939)
XLA Ops:
  0.0 57.5 %layer.1 = bf16[128,256]{1,0:T(8,128)(2,1)} custom-call(bf16[128,256]{1,0:T(8,128)(2,1)} %residual.1, bf16[128,128]{1,0:T(8,128)(2,1)} %lifted.1, f32[8,128]{1,0:T(8,128)} %pace.1, f32[8,128]{1,0:T(8,128)} %fading.1, f32[2,32,64]{2,1,0:T(8,128)} %rate_l.1, f32[2,32,32]{2,1,0:T(8,128)} %rate_s.1, f32[2,32,64]{2,1,0:T(8,128)} %turn_l.1, f32[2,32,32]{2,1,0:T(8,128)} %turn_s.1, ...), custom_call_target="tpu_custom_call" | custom-call | tf_op jit(solution)/shard_map/layer/pallas_call | solution.py:564
  57.5 1.5 %copy.18 = bf16[128,256]{1,0:T(8,128)(2,1)} copy(bf16[128,256]{1,0:T(8,128)(2,1)} %layer.1) | data formatting | bytes 131072

commit v3 on v2

--- a/solution.py
+++ b/solution.py
@@ -75,7 +75,7 @@
     maps_v, pace_s, fading_s, drive_s, prefix_s, state_s, lifted_s,
     ends, cx, cz, row_ends, merged_v, gathered, res_v, mid_v, mid_f, own_mid,
     weights, hidden, partial, from_y, from_x, sum_y, sum_x, final,
-    load_sem, up_send, up_recv, down_send, down_recv, cx_send, cx_recv, cz_send, cz_recv,
+    load_sem, up_send, up_recv, down_recv, cx_send, cx_recv, cz_send, cz_recv,
     mg_send, mg_recv, ay_send, ay_recv, ax_send, ax_recv, fy_send, fx_send, final_recv, res_send, res_recv, ring_send, ring_recv,
     sib_send, sib_recv, mid_send, mid_recv,
 ):
@@ -97,20 +97,6 @@
     def arrival(ref, sem):
         pltpu.make_async_copy(ref, ref, sem).wait()
 
-    barrier = pltpu.get_barrier_semaphore()
-    spot = x * 8 + tp
-
-    @pl.loop(1, 32)
-    def _(off):
-        to = (spot + off) % 32
-        pl.semaphore_signal(barrier, inc=1, device_id=(z * NX + to // 8, to % 8), device_id_type=MESH)
-
-    @pl.loop(1, NZ)
-    def _(off):
-        pl.semaphore_signal(
-            barrier, inc=1, device_id=(((z + off) % NZ) * NX + x, tp), device_id_type=MESH
-        )
-
     loads = [
         (lifted, lifted_v), (pace, pace_v), (fading, fading_v), (rate_l, rate_lv),
         (rate_s, rate_sv), (turn_l, turn_lv), (turn_s, turn_sv),
@@ -122,6 +108,21 @@
     copies = [pltpu.make_async_copy(a, b, load_sem.at[n]) for n, (a, b) in enumerate(loads)]
     for copy in copies:
         copy.start()
+
+    barrier = pltpu.get_barrier_semaphore()
+    spot = x * 8 + tp
+
+    @pl.loop(1, 32)
+    def _(off):
+        to = (spot + off) % 32
+        pl.semaphore_signal(barrier, inc=1, device_id=(z * NX + to // 8, to % 8), device_id_type=MESH)
+
+    @pl.loop(1, NZ)
+    def _(off):
+        pl.semaphore_signal(
+            barrier, inc=1, device_id=(((z + off) % NZ) * NX + x, tp), device_id_type=MESH
+        )
+
     for copy in copies[:-4]:
         copy.wait()
 
@@ -170,34 +171,6 @@
         for part in range(2):
             drive_s[e, part] = mm(lifted_b, maps_v[e, 0, part, 0]) + mm(lifted_b, maps_v[e, 0, part, 1])
 
-    copies[-4].wait()
-    copies[-3].wait()
-    pl.semaphore_wait(barrier, 31 + NZ - 1)
-
-    sends = []
-
-    def begin(copy):
-        copy.start()
-        sends.append(copy)
-
-    def pieces(off):
-        xt = (x + off) % NX
-        up_src = raising_v.at[:, pl.ds(pl.multiple_of(xt * 256, 256), 256)]
-        up_dst = weights.at[0, z, c, pl.ds(x * 64, 64), :]
-        down_src = lowering_v.at[:, pl.ds(pl.multiple_of(xt * 256, 256), 256)]
-        down_dst = weights.at[1, z, c, pl.ds(x * 64, 64), :]
-        return xt, up_src, up_dst, down_src, down_dst
-
-    for off in (2, 1, 3):
-        xt, src, dst, _, _ = pieces(off)
-        begin(remote(src, dst, up_send.at[off], up_recv, (z * NX + xt, tp)))
-    for off in (2, 1, 3):
-        xt, _, _, src, dst = pieces(off)
-        begin(remote(src, dst, down_send.at[off], down_recv, (z * NX + xt, tp)))
-    _, up_src, up_dst, down_src, down_dst = pieces(0)
-    pltpu.make_async_copy(up_src, up_dst, up_recv).start()
-    pltpu.make_async_copy(down_src, down_dst, down_recv).start()
-
     def step(s, carry):
         new = []
         for e in range(2):
@@ -220,7 +193,35 @@
         return tuple(new)
 
     one, zero = jnp.ones((8, ST), F32), jnp.zeros((8, ST), F32)
-    tops = lax.fori_loop(0, STEPS, step, (one, zero, zero, zero) * 2)
+    tops = lax.fori_loop(0, STEPS // 2, step, (one, zero, zero, zero) * 2)
+
+    copies[-4].wait()
+    copies[-3].wait()
+    pl.semaphore_wait(barrier, 31 + NZ - 1)
+
+
+    def begin(copy):
+        copy.start()
+
+    def pieces(off):
+        xt = (x + off) % NX
+        up_src = raising_v.at[:, pl.ds(pl.multiple_of(xt * 256, 256), 256)]
+        up_dst = weights.at[0, z, c, pl.ds(x * 64, 64), :]
+        down_src = lowering_v.at[:, pl.ds(pl.multiple_of(xt * 256, 256), 256)]
+        down_dst = weights.at[1, z, c, pl.ds(x * 64, 64), :]
+        return xt, up_src, up_dst, down_src, down_dst
+
+    for off in (2, 1, 3):
+        xt, src, dst, _, _ = pieces(off)
+        begin(remote(src, dst, up_send, up_recv, (z * NX + xt, tp)))
+    for off in (2, 1, 3):
+        xt, _, _, src, dst = pieces(off)
+        begin(remote(src, dst, up_send, down_recv, (z * NX + xt, tp)))
+    _, up_src, up_dst, down_src, down_dst = pieces(0)
+    pltpu.make_async_copy(up_src, up_dst, up_recv).start()
+    pltpu.make_async_copy(down_src, down_dst, down_recv).start()
+
+    tops = lax.fori_loop(STEPS // 2, STEPS, step, tops)
 
     def composed(first, later):
         fre, fim, bre, bim = first
@@ -246,9 +247,8 @@
     cx[x] = own_ends
 
     for off in (2, 1, 3):
-        copy = remote(ends, cx.at[x], cx_send.at[off], cx_recv, (z * NX + (x + off) % NX, tp))
+        copy = remote(ends, cx.at[x], cx_send, cx_recv, (z * NX + (x + off) % NX, tp))
         copy.start()
-        sends.append(copy)
     ORDER = (
         (0, 0, 0), (0, 1, 0), (1, 0, 0), (0, 0, 1), (0, 1, 1), (1, 1, 0), (0, 0, 2),
         (0, 1, 2), (1, 0, 1), (0, 0, 3), (1, 1, 1), (1, 0, 2), (1, 1, 2), (1, 0, 3),
@@ -260,20 +260,20 @@
         zs = (z + (NZ - hops if way == 0 else hops)) % NZ
         return kind, weights.at[kind, zs, c, pl.ds((half ^ way) * 128, 128), :]
 
-    def share(kind, ref, slot):
-        begin(remote(ref, ref, sib_send.at[slot], sib_recv.at[kind], (sp, sib)))
+    def share(kind, ref):
+        begin(remote(ref, ref, sib_send, sib_recv.at[kind], (sp, sib)))
 
     def ring_send_slot(slot):
         for way in range(2):
             to = ((z + (1 if way == 0 else NZ - 1)) % NZ) * NX + x
             _, ref = piece(way, slot, 0)
-            begin(remote(ref, ref, ring_send.at[way, slot], ring_recv.at[way, slot], (to, tp)))
+            begin(remote(ref, ref, ring_send, ring_recv.at[way, slot], (to, tp)))
 
     def ring_take(slot):
         for way in range(2):
             kind, ref = piece(way, slot, 1)
             arrival(ref, ring_recv.at[way, slot])
-            share(kind, ref, 2 + 2 * slot + way)
+            share(kind, ref)
 
     own_block = pl.ds(pl.multiple_of(inner * TOK, TOK), TOK)
 
@@ -284,7 +284,7 @@
     def to_plane(src, dst, send, recv):
         @pl.loop(1, NX * NY)
         def _(off):
-            remote(src, dst, send.at[off], recv, plane(off)).start()
+            remote(src, dst, send.at[0], recv, plane(off)).start()
 
         @pl.when(c == block)
         def _():
@@ -292,48 +292,46 @@
 
         @pl.when(c != block)
         def _():
-            remote(src, dst, send.at[0], recv, plane(0)).start()
-
-    def plane_sent(src, dst, send, recv):
-        @pl.loop(1, NX * NY)
-        def _(off):
-            remote(src, dst, send.at[off], recv, plane(off)).wait_send()
+            remote(src, dst, send.at[1], recv, plane(0)).start()
+
+    def plane_sent(src, dst, send, recv, fifteen):
+        arrival(fifteen, send.at[0])
 
         @pl.when(c != block)
         def _():
-            remote(src, dst, send.at[0], recv, plane(0)).wait_send()
+            remote(src, dst, send.at[1], recv, plane(0)).wait_send()
 
     res_dst = res_v.at[own_block, pl.ds(pl.multiple_of(tp * 256, 256), 256)]
     arrival(weights.at[0, z, c], up_recv)
     ring_send_slot(0)
     ring_send_slot(1)
-    share(0, weights.at[0, z, c], 0)
+    share(0, weights.at[0, z, c])
+    to_plane(residual, res_dst, res_send, res_recv)
+
     arrival(cx.at[pl.ds(0, NX - 1)], cx_recv)
 
-    def as_map(ref, n, e):
-        return tuple(ref[n, 4 * e + q : 4 * e + q + 1, :] for q in range(4))
+    def as_map(ref, n, top):
+        return tuple(ref[n, top + q : top + q + 1, :] for q in range(4))
 
     row = []
     for e in range(2):
         run = unit
         for n in range(NX) if e == 0 else reversed(range(NX)):
-            run = composed(run, as_map(cx, n, e))
+            run = composed(run, as_map(cx, n, 4 * e))
         row += list(run)
-    row_total = jnp.concatenate(row, axis=0)
-    row_ends[...] = row_total
-    cz[z] = row_total
+    row_ends[0] = jnp.concatenate(row[:4], axis=0)
+    row_ends[1] = jnp.concatenate(row[4:], axis=0)
+    cz[z] = jnp.concatenate(row[:4], axis=0)
     for off in (4, 3, 5, 2, 6, 1, 7):
         copy = remote(
-            row_ends, cz.at[z], cz_send.at[off], cz_recv, (((z + off) % NZ) * NX + x, tp)
+            row_ends.at[jnp.where(z + off < NZ, 0, 1)], cz.at[z], cz_send, cz_recv,
+            (((z + off) % NZ) * NX + x, tp),
         )
         copy.start()
-        sends.append(copy)
 
     arrival(weights.at[1, z, c], down_recv)
     ring_send_slot(2)
-    share(1, weights.at[1, z, c], 1)
-    to_plane(residual, res_dst, res_send, res_recv)
-
+    share(1, weights.at[1, z, c])
     ring_take(0)
     ring_send_slot(3)
     ring_take(1)
@@ -351,10 +349,10 @@
     out_y = jnp.zeros((TOK, CH), F32)
     for e in range(2):
         state = (blank, blank)
-        for ref, count, at in ((cz, NZ, z), (cx, NX, x)):
+        for ref, count, at, top in ((cz, NZ, z, 0), (cx, NX, x, 4 * e)):
             for n in range(count) if e == 0 else reversed(range(count)):
                 passed = (n < at) if e == 0 else (n > at)
-                new = applied(as_map(ref, n, e), state)
+                new = applied(as_map(ref, n, top), state)
                 state = tuple(jnp.where(passed, a, b) for a, b in zip(new, state))
         entry = applied(before[e], state)
         tall = tuple(jnp.concatenate([v] * STEPS, axis=0) for v in entry)
@@ -397,7 +395,6 @@
     copies[-1].wait()
     copies[-2].wait()
     arrival(res_v, res_recv)
-    ring_take(12)
     arrival(gathered, mg_recv)
 
     def project(n, squares):
@@ -408,7 +405,7 @@
         return squares + jnp.sum(m * m, axis=1, keepdims=True)
 
     squares = lax.fori_loop(0, 2, project, jnp.zeros((2 * TOK, 1), F32))
-    ring_take(13)
+    ring_take(12)
     squares = lax.fori_loop(2, 4, project, squares)
     scale = lax.rsqrt(squares * (1.0 / D) + EPSILON)
 
@@ -424,11 +421,13 @@
         up = mm(mid_v[...], weights[0, :, n].reshape(D, 256)) * scale
         up = jnp.maximum(up, 0.0)
         hidden[:, n * 256 : (n + 1) * 256] = (up * up).astype(BF16)
+    ring_take(13)
     arrival(weights.at[1, :, 1 - c], sib_recv.at[1])
 
-    def down(n):
-        both = nt(hidden[:, :256], weights[1, n, 0]) + nt(hidden[:, 256:], weights[1, n, 1])
-        partial[n] = both.astype(BF16)
+    def down(*ns):
+        both = [nt(hidden[:, :256], weights[1, n, 0]) + nt(hidden[:, 256:], weights[1, n, 1]) for n in ns]
+        for n, value in zip(ns, both):
+            partial[n] = value.astype(BF16)
 
     def row_of(k):
         return (y + 1 + k) % NY
@@ -437,13 +436,13 @@
         to = row_of(k)
         src = partial.at[2 * to + 1, pl.ds(i * TOK, TOK), :]
         dst = from_y.at[i, y]
-        return src, dst, remote(src, dst, ay_send.at[i, k], ay_recv.at[i], (sp, 2 * to + c))
+        return src, dst, remote(src, dst, ay_send, ay_recv.at[i], (sp, 2 * to + c))
 
     def along_x(k, i):
         src = partial.at[2 * row_of(k), pl.ds(i * TOK, TOK), :]
         dst = from_x.at[row_of(k), x]
         to = (z * NX + 2 * c + i, tp)
-        return src, dst, remote(src, dst, ax_send.at[k, i], ax_recv.at[k], to)
+        return src, dst, remote(src, dst, ax_send, ax_recv.at[k], to)
 
     def on_y(i):
         dst = final.at[x]
@@ -484,19 +483,21 @@
     def local_y(k):
         return (c == 0) if k == NY - 1 else None
 
-    for k in range(NY):
-        down(2 * row_of(k) + 1)
+    for k in (0, 2, 1, 3):
+        down(2 * row_of(k) + 1, 2 * row_of(k))
         if k < NY - 1:
             along_y(0, k)[2].start()
         else:
             for i in range(2):
                 src, dst, _ = along_y(i, k)
                 pltpu.make_async_copy(src, dst, ay_recv.at[i]).start()
-        down(2 * row_of(k))
         for i in range(2):
             deliver(along_x(k, i), ax_recv.at[k], near(i))
-    for k in range(NY - 1):
-        along_y(1, k)[2].start()
+        if k == 2:
+            for n in (0, 2):
+                along_y(1, n)[2].start()
+        if k == 1:
+            along_y(1, k)[2].start()
 
     def summed(ref):
         total = ref[0].astype(F32)
@@ -522,16 +523,19 @@
         own_mid_copy.start()
 
     turn_x(0)
+    turn_x(2)
     turn_y(0)
     turn_x(1)
-    turn_x(2)
     turn_x(3)
     turn_y(1)
 
-    for copy in sends:
-        copy.wait_send()
-    plane_sent(residual, res_dst, res_send, res_recv)
-    plane_sent(merged_v, mg_dst, mg_send, mg_recv)
+    arrival(hidden.at[pl.ds(0, 192), :], up_send)
+    arrival(cx.at[pl.ds(0, NX - 1)], cx_send)
+    arrival(cz.at[pl.ds(0, NZ - 1)], cz_send)
+    arrival(weights.at[0, pl.ds(0, 7)], ring_send)
+    arrival(weights.at[0], sib_send)
+    plane_sent(residual, res_dst, res_send, res_recv, res_v.at[pl.ds(0, 240), :])
+    plane_sent(merged_v, mg_dst, mg_send, mg_recv, gathered.at[pl.ds(0, 240), :])
 
     @pl.when(c == block)
     def _():
@@ -541,15 +545,17 @@
     arrival(final, final_recv)
     out[...] = (own_mid[...] + summed(final)).astype(BF16)
 
-    for k in range(NY):
-        for i in range(2):
-            delivered(along_x(k, i), near(i))
-            if k < NY - 1:
-                along_y(i, k)[2].wait_send()
-
-        @pl.when(c == block)
-        def _():
+    arrival(partial.at[pl.ds(0, 3)], ay_send)
+
+    @pl.when(c == block)
+    def _():
+        arrival(partial.at[pl.ds(0, 2)], ax_send)
+        for k in range(NY):
             delivered(on_x(k), local_y(k))
+
+    @pl.when(c != block)
+    def _():
+        arrival(partial.at[pl.ds(0, 4)], ax_send)
 
     for i in range(2):
         delivered(on_y(i), jnp.logical_and(near(i), c == 1))
@@ -563,7 +569,7 @@
     vm = pltpu.VMEM
     return pl.pallas_call(
         kernel,
-        out_shape=jax.ShapeDtypeStruct((TOK, 256), BF16),
+        out_shape=pltpu.VMEM((TOK, 256), BF16),
         in_specs=[pl.BlockSpec(memory_space=pl.ANY)] * 16,
         out_specs=pl.BlockSpec(memory_space=pltpu.VMEM),
         scratch_shapes=[
@@ -574,15 +580,15 @@
             vm((2, 2, 2, 2, CH, ST), BF16), vm((TOK, ST), F32), vm((TOK, ST), F32),
             vm((2, 2, TOK, ST), F32), vm((2, 2, TOK, ST), F32), vm((2, 2, TOK, ST), F32),
             vm((TOK, CH), F32),
-            vm((8, ST), F32), vm((NX, 8, ST), F32), vm((NZ, 8, ST), F32), vm((8, ST), F32),
+            vm((8, ST), F32), vm((NX, 8, ST), F32), vm((NZ, 4, ST), F32), vm((2, 4, ST), F32),
             vm((TOK, CH), BF16), vm((2 * TOK, 1024), BF16), vm((2 * TOK, D), BF16),
             vm((2 * TOK, D), BF16), vm((2 * TOK, D), F32), vm((TOK, 256), F32),
             vm((2, NZ, 2, 256, 256), BF16), vm((2 * TOK, 512), BF16),
             vm((8, 2 * TOK, 256), BF16), vm((2, NY, TOK, 256), BF16), vm((NY, NX, TOK, 256), BF16),
             vm((2, TOK, 256), BF16), vm((NY, TOK, 256), BF16), vm((4, TOK, 256), BF16),
-            dma((15,)), dma((NX,)), dma, dma((NX,)), dma, dma((NX,)), dma, dma((NZ,)), dma,
-            dma((16,)), dma, dma((2, 4)), dma((2,)), dma((4, 2)), dma((4,)), dma((2,)), dma((4,)), dma, dma((16,)), dma, dma((2, 14)), dma((2, 14)),
-            dma((30,)), dma((2,)), dma, dma,
+            dma((15,)), dma, dma, dma, dma, dma, dma, dma,
+            dma((2,)), dma, dma, dma((2,)), dma, dma((4,)), dma((2,)), dma((4,)), dma,
+            dma((2,)), dma, dma, dma((2, 14)), dma, dma((2,)), dma, dma,
         ],
         compiler_params=pltpu.CompilerParams(
             collective_id=0, has_side_effects=True, vmem_limit_bytes=60 * 1024 * 1024

time: 59.1 us -> 54.1 us (0.915)
  the two profiles are of different devices: /device:TPU:3 before, /device:TPU:1 now
where the time goes in v3:
time: 54.1 us; the launch traced here: 54 us
  Pallas kernels  53.4 us (99%)
  local copies, waits for them, and re-layouts  0.63 us (1%)
    pallas_call x1, Pallas kernels, on_device(): pl.pallas_call(kernel, out_shape=pltpu.VMEM((TOK, 256), BF16), in_specs=[...  53.4 us

profile of v3, /device:TPU:1, one launch (start us, length us, event | category | flops | bytes accessed | tf_op | source)
XLA Modules:
  0.0 54.0 jit_solution(14518402881286360377)
XLA Ops:
  0.0 53.4 %layer.1 = bf16[128,256]{1,0:T(8,128)(2,1)S(1)} custom-call(bf16[128,256]{1,0:T(8,128)(2,1)} %residual.1, bf16[128,128]{1,0:T(8,128)(2,1)} %lifted.1, f32[8,128]{1,0:T(8,128)} %pace.1, f32[8,128]{1,0:T(8,128)} %fading.1, f32[2,32,64]{2,1,0:T(8,128)} %rate_l.1, f32[2,32,32]{2,1,0:T(8,128)} %rate_s.1, f32[2,32,64]{2,1,0:T(8,128)} %turn_l.1, ...), custom_call_target="tpu_custom_call" | custom-call | tf_op jit(solution)/shard_map/layer/pallas_call | solution.py:570
  53.4 0.6 %copy.18 = bf16[128,256]{1,0:T(8,128)(2,1)} copy(bf16[128,256]{1,0:T(8,128)(2,1)S(1)} %layer.1) | data formatting | bytes 131072

commit v4 on v3

--- a/solution.py
+++ b/solution.py
@@ -112,16 +112,13 @@
     barrier = pltpu.get_barrier_semaphore()
     spot = x * 8 + tp
 
-    @pl.loop(1, 32)
-    def _(off):
-        to = (spot + off) % 32
-        pl.semaphore_signal(barrier, inc=1, device_id=(z * NX + to // 8, to % 8), device_id_type=MESH)
-
-    @pl.loop(1, NZ)
-    def _(off):
+    for off in (4, 3, 5, 2, 6, 1, 7):
         pl.semaphore_signal(
             barrier, inc=1, device_id=(((z + off) % NZ) * NX + x, tp), device_id_type=MESH
         )
+    for off in sorted(range(1, 32), key=lambda n: abs(n - 16)):
+        to = (spot + off) % 32
+        pl.semaphore_signal(barrier, inc=1, device_id=(z * NX + to // 8, to % 8), device_id_type=MESH)
 
     for copy in copies[:-4]:
         copy.wait()
@@ -214,12 +211,9 @@
     for off in (2, 1, 3):
         xt, src, dst, _, _ = pieces(off)
         begin(remote(src, dst, up_send, up_recv, (z * NX + xt, tp)))
-    for off in (2, 1, 3):
-        xt, _, _, src, dst = pieces(off)
-        begin(remote(src, dst, up_send, down_recv, (z * NX + xt, tp)))
     _, up_src, up_dst, down_src, down_dst = pieces(0)
     pltpu.make_async_copy(up_src, up_dst, up_recv).start()
-    pltpu.make_async_copy(down_src, down_dst, down_recv).start()
+
 
     tops = lax.fori_loop(STEPS // 2, STEPS, step, tops)
 
@@ -249,9 +243,14 @@
     for off in (2, 1, 3):
         copy = remote(ends, cx.at[x], cx_send, cx_recv, (z * NX + (x + off) % NX, tp))
         copy.start()
+    for off in (2, 1, 3):
+        xt, _, _, src, dst = pieces(off)
+        begin(remote(src, dst, up_send, down_recv, (z * NX + xt, tp)))
+    pltpu.make_async_copy(down_src, down_dst, down_recv).start()
+
     ORDER = (
-        (0, 0, 0), (0, 1, 0), (1, 0, 0), (0, 0, 1), (0, 1, 1), (1, 1, 0), (0, 0, 2),
-        (0, 1, 2), (1, 0, 1), (0, 0, 3), (1, 1, 1), (1, 0, 2), (1, 1, 2), (1, 0, 3),
+        (0, 0, 0), (0, 1, 0), (1, 0, 0), (1, 1, 0), (0, 0, 1), (0, 1, 1), (1, 0, 1),
+        (1, 1, 1), (0, 0, 2), (0, 1, 2), (1, 0, 2), (1, 1, 2), (0, 0, 3), (1, 0, 3),
     )
 
     def piece(way, slot, extra):
@@ -304,7 +303,6 @@
     res_dst = res_v.at[own_block, pl.ds(pl.multiple_of(tp * 256, 256), 256)]
     arrival(weights.at[0, z, c], up_recv)
     ring_send_slot(0)
-    ring_send_slot(1)
     share(0, weights.at[0, z, c])
     to_plane(residual, res_dst, res_send, res_recv)
 
@@ -329,16 +327,19 @@
         )
         copy.start()
 
+    ring_send_slot(1)
     arrival(weights.at[1, z, c], down_recv)
     ring_send_slot(2)
+    ring_send_slot(3)
     share(1, weights.at[1, z, c])
     ring_take(0)
-    ring_send_slot(3)
+    ring_send_slot(4)
     ring_take(1)
-    ring_send_slot(4)
     ring_send_slot(5)
 
     arrival(cz.at[pl.ds(0, NZ - 1)], cz_recv)
+    ring_take(2)
+    ring_send_slot(6)
 
     def applied(m, state):
         pre, pim, hre, him = m
@@ -374,39 +375,37 @@
     mg_dst = gathered.at[own_block, pl.ds(pl.multiple_of(tp * CH, CH), CH)]
     to_plane(merged_v, mg_dst, mg_send, mg_recv)
 
-    ring_take(2)
     ring_take(3)
-    ring_send_slot(6)
+    ring_send_slot(7)
     ring_take(4)
-    ring_send_slot(7)
     ring_send_slot(8)
     ring_take(5)
+    ring_send_slot(9)
     ring_take(6)
-    ring_send_slot(9)
     ring_send_slot(10)
     ring_take(7)
+    ring_send_slot(11)
     ring_take(8)
-    ring_send_slot(11)
+    ring_send_slot(12)
     ring_take(9)
     ring_take(10)
-    ring_send_slot(12)
+    ring_send_slot(13)
     ring_take(11)
-    ring_send_slot(13)
     copies[-1].wait()
     copies[-2].wait()
     arrival(res_v, res_recv)
     arrival(gathered, mg_recv)
 
     def project(n, squares):
-        cols = pl.ds(pl.multiple_of(n * 512, 512), 512)
+        cols = pl.ds(n * 1024, 1024)
         m = mm(gathered[...], emitted_v[:, cols]) + res_v[:, cols].astype(F32)
         mid_f[:, cols] = m
         mid_v[:, cols] = (m * leading_v[:, cols]).astype(BF16)
         return squares + jnp.sum(m * m, axis=1, keepdims=True)
 
-    squares = lax.fori_loop(0, 2, project, jnp.zeros((2 * TOK, 1), F32))
+    squares = project(0, jnp.zeros((2 * TOK, 1), F32))
     ring_take(12)
-    squares = lax.fori_loop(2, 4, project, squares)
+    squares = project(1, squares)
     scale = lax.rsqrt(squares * (1.0 / D) + EPSILON)
 
     own_cols = pl.ds(pl.multiple_of(tp * 256, 256), 256)
@@ -416,12 +415,12 @@
     def _():
         remote(mid_f.at[own_block, sib_cols], own_mid, mid_send, mid_recv, (sp, sib)).start()
 
+    ring_take(13)
     arrival(weights.at[0, :, 1 - c], sib_recv.at[0])
     for n in range(2):
         up = mm(mid_v[...], weights[0, :, n].reshape(D, 256)) * scale
         up = jnp.maximum(up, 0.0)
         hidden[:, n * 256 : (n + 1) * 256] = (up * up).astype(BF16)
-    ring_take(13)
     arrival(weights.at[1, :, 1 - c], sib_recv.at[1])
 
     def down(*ns):
@@ -483,7 +482,7 @@
     def local_y(k):
         return (c == 0) if k == NY - 1 else None
 
-    for k in (0, 2, 1, 3):
+    for k in (1, 0, 2, 3):
         down(2 * row_of(k) + 1, 2 * row_of(k))
         if k < NY - 1:
             along_y(0, k)[2].start()
@@ -494,10 +493,8 @@
         for i in range(2):
             deliver(along_x(k, i), ax_recv.at[k], near(i))
         if k == 2:
-            for n in (0, 2):
+            for n in (1, 0, 2):
                 along_y(1, n)[2].start()
-        if k == 1:
-            along_y(1, k)[2].start()
 
     def summed(ref):
         total = ref[0].astype(F32)
@@ -522,11 +519,11 @@
         own_mid_copy = pltpu.make_async_copy(mid_f.at[own_block, own_cols], own_mid, mid_recv)
         own_mid_copy.start()
 
+    turn_x(1)
     turn_x(0)
     turn_x(2)
+    turn_x(3)
     turn_y(0)
-    turn_x(1)
-    turn_x(3)
     turn_y(1)
 
     arrival(hidden.at[pl.ds(0, 192), :], up_send)

time: 54.1 us -> 53.1 us (0.982)
  Pallas kernels: 53.4 us -> 52.3 us
    pallas_call x1, Pallas kernels: 53.4 us -> 52.3 us  [on_device(): pl.pallas_call(kernel, out_shape=pltpu.VMEM((TOK, 256), BF16), in_specs=[...]
where the time goes in v4:
time: 53.1 us; the launch traced here: 53 us
  Pallas kernels  52.3 us (98%)
  local copies, waits for them, and re-layouts  0.63 us (1%)
    pallas_call x1, Pallas kernels, on_device(): pl.pallas_call(kernel, out_shape=pltpu.VMEM((TOK, 256), BF16), in_specs=[...  52.3 us

profile of v4, /device:TPU:1, one launch (start us, length us, event | category | flops | bytes accessed | tf_op | source)
XLA Modules:
  0.0 53.0 jit_solution(2581366375540617070)
XLA Ops:
  0.0 52.3 %layer.1 = bf16[128,256]{1,0:T(8,128)(2,1)S(1)} custom-call(bf16[128,256]{1,0:T(8,128)(2,1)} %residual.1, bf16[128,128]{1,0:T(8,128)(2,1)} %lifted.1, f32[8,128]{1,0:T(8,128)} %pace.1, f32[8,128]{1,0:T(8,128)} %fading.1, f32[2,32,64]{2,1,0:T(8,128)} %rate_l.1, f32[2,32,32]{2,1,0:T(8,128)} %rate_s.1, f32[2,32,64]{2,1,0:T(8,128)} %turn_l.1, ...), custom_call_target="tpu_custom_call" | custom-call | tf_op jit(solution)/shard_map/layer/pallas_call | solution.py:567
  52.4 0.6 %copy.18 = bf16[128,256]{1,0:T(8,128)(2,1)} copy(bf16[128,256]{1,0:T(8,128)(2,1)S(1)} %layer.1) | data formatting | bytes 131072

commit v5 on v4

--- a/solution.py
+++ b/solution.py
@@ -150,9 +150,10 @@
     tile_s = one_hot(iota((32, CH), 0) == (iota((32, CH), 1) & 31)).astype(BF16)
     own_l = (iota((64, LONG), 0) >> 4) == (iota((64, LONG), 1) >> 6)
     own_s = (iota((64, CH), 0) >> 4) == (iota((64, CH), 1) >> 5)
-    maps_v[...] = jnp.zeros(maps_v.shape, BF16)
-    for e in range(2):
-        for io in range(2):
+
+    def build_maps(io):
+        maps_v[:, io] = jnp.zeros((2, 2, 2, CH, ST), BF16)
+        for e in range(2):
             for part in range(2):
                 wide = halves(proj_lv[e, io, part].reshape(64, 64))
                 slim = halves(proj_sv[e, io, part].reshape(64, 32))
@@ -163,6 +164,8 @@
                         rows = slice(16 * n, 16 * n + 16)
                         maps_v[e, io, part, h, 32 * n : 32 * n + 16, :LONG] = a[rows]
                         maps_v[e, io, part, h, 32 * n + 16 : 32 * n + 32, LONG:] = b[rows]
+
+    build_maps(0)
     lifted_b = lifted_p.astype(BF16)
     for e in range(2):
         for part in range(2):
@@ -190,7 +193,7 @@
         return tuple(new)
 
     one, zero = jnp.ones((8, ST), F32), jnp.zeros((8, ST), F32)
-    tops = lax.fori_loop(0, STEPS // 2, step, (one, zero, zero, zero) * 2)
+    tops = lax.fori_loop(0, STEPS // 4, step, (one, zero, zero, zero) * 2)
 
     copies[-4].wait()
     copies[-3].wait()
@@ -215,7 +218,7 @@
     pltpu.make_async_copy(up_src, up_dst, up_recv).start()
 
 
-    tops = lax.fori_loop(STEPS // 2, STEPS, step, tops)
+    tops = lax.fori_loop(STEPS // 4, STEPS, step, tops)
 
     def composed(first, later):
         fre, fim, bre, bim = first
@@ -301,6 +304,8 @@
             remote(src, dst, send.at[1], recv, plane(0)).wait_send()
 
     res_dst = res_v.at[own_block, pl.ds(pl.multiple_of(tp * 256, 256), 256)]
+    build_maps(1)
+
     arrival(weights.at[0, z, c], up_recv)
     ring_send_slot(0)
     share(0, weights.at[0, z, c])

time: 53.1 us -> 52.6 us (level)
  no operation moved by 1% of the time
where the time goes in v5:
time: 52.6 us; the launch traced here: 52.5 us
  Pallas kernels  51.9 us (99%)
  local copies, waits for them, and re-layouts  0.63 us (1%)
    pallas_call x1, Pallas kernels, on_device(): pl.pallas_call(kernel, out_shape=pltpu.VMEM((TOK, 256), BF16), in_specs=[...  51.9 us

profile of v5, /device:TPU:1, one launch (start us, length us, event | category | flops | bytes accessed | tf_op | source)
XLA Modules:
  0.0 52.5 jit_solution(14896925302090930031)
XLA Ops:
  0.0 51.9 %layer.1 = bf16[128,256]{1,0:T(8,128)(2,1)S(1)} custom-call(bf16[128,256]{1,0:T(8,128)(2,1)} %residual.1, bf16[128,128]{1,0:T(8,128)(2,1)} %lifted.1, f32[8,128]{1,0:T(8,128)} %pace.1, f32[8,128]{1,0:T(8,128)} %fading.1, f32[2,32,64]{2,1,0:T(8,128)} %rate_l.1, f32[2,32,32]{2,1,0:T(8,128)} %rate_s.1, f32[2,32,64]{2,1,0:T(8,128)} %turn_l.1, ...), custom_call_target="tpu_custom_call" | custom-call | tf_op jit(solution)/shard_map/layer/pallas_call | solution.py:572
  51.9 0.6 %copy.18 = bf16[128,256]{1,0:T(8,128)(2,1)} copy(bf16[128,256]{1,0:T(8,128)(2,1)S(1)} %layer.1) | data formatting | bytes 131072
